TPU v7x, 512 devices: a 4x2x32 block of a 4x8x32 slice. The times are simulated.
512 devices in a mesh: grp: 2 (over y), sp: 32 (over z), tp: 8 (over x, core).
Axes of the slice: x: 4, y: 2, z: 32, core: 2. Of those that a mesh axis runs over, the one named last changes fastest.
The devices are a block of a 4x8x32 slice.
Arguments:
- tokens: bfloat16 [8192, 2048], P(('grp', 'sp')), parts along dimension 0, may hold values from -8 to 8
- norm_gain: float32 [2048], replicated, may hold values from 0.1 to 1.9
- w_query: bfloat16 [2048, 1024], P(None, 'tp'), may hold values from -0.125 to 0.125
- w_key: bfloat16 [2048, 1024], P(None, 'tp'), may hold values from -0.125 to 0.125
- w_value: bfloat16 [2048, 1024], P(None, 'tp'), may hold values from -0.125 to 0.125
- w_out: bfloat16 [1024, 2048], P('tp'), may hold values from -0.1875 to 0.1875
- key_rate: bfloat16 [16, 8192], P('tp', ('grp', 'sp')), parts along dimension 1, may hold values from -16 to 1
Outputs:
- layer_out: bfloat16 [8192, 2048], P(('grp', 'sp')), parts along dimension 0
There are 2 independent parts, one for each index of `grp`. A program takes and returns all parts, laid end to end along the dimension named above; an argument that names none is the same for every part. Nothing has to cross between parts.
All inputs are finite; a program needn't handle non-finite values.
Results may differ from a plain program's by a relative error of at most 0.0075.
Values may be sent and summed in bfloat16 or wider, within the bound.
A program may use at most 64 MiB of HBM per device.

v0:
```python
import jax
import jax.numpy as jnp
from jax import lax
from jax.sharding import PartitionSpec as P

HD = 64
KEY_SPAN = 128


F32 = jnp.float32
BF16 = jnp.bfloat16
EPS = 1e-06


def sent_together(arrays, axis, dim, along):
    ends, at = ([], 0)
    for a in arrays[:-1]:
        at += a.shape[along]
        ends.append(at)
    both = jnp.concatenate(arrays, axis=along)
    return tuple(jnp.split(lax.all_gather(both, axis, axis=dim, tiled=True), ends, axis=along))


def from_everyone(shard, axis):
    count = lax.axis_size(axis)
    return lax.all_to_all(
        jnp.broadcast_to(shard[None], (count, *shard.shape)), axis, 0, 0, tiled=True
    )


def laid_out(parts, dim):
    dims = list(parts.shape[1:])
    dims[dim] *= parts.shape[0]
    return jnp.moveaxis(parts, 0, dim).reshape(dims)


def gather_directly(shard, axis, dim):
    parts = from_everyone(shard, axis)
    return laid_out(parts, dim)


def break_scores(query_heads, key_heads, rate_row_values, query_pos, key_pos):
    scores = jnp.einsum(
        "qhd,khd->hqk", query_heads, key_heads, preferred_element_type=F32
    ) * HD ** (-0.5)
    scores = scores + jnp.transpose(rate_row_values).astype(F32)[:, None, :]
    causal_mask = key_pos[None, :] < query_pos[:, None]
    log_remain = jnp.where(causal_mask[None], jax.nn.log_sigmoid(-scores), 0.0)
    return (scores, causal_mask, log_remain)


def shard_summary(query_heads, key_heads, value_heads, rate_row_values, query_pos, key_pos):
    scores, causal_mask, log_remain = break_scores(
        query_heads, key_heads, rate_row_values, query_pos, key_pos
    )
    heads_here, query_count, key_count = scores.shape
    span_count = key_count // KEY_SPAN
    blocks = log_remain.reshape(heads_here, query_count, span_count, KEY_SPAN)
    span_ids = jnp.arange(KEY_SPAN, dtype=jnp.int32)
    tri_strict = (span_ids[:, None] > span_ids[None, :]).astype(F32)
    inside_sum = jnp.einsum("hqnj,js->hqns", blocks, tri_strict)
    block_ids = jnp.arange(span_count, dtype=jnp.int32)
    block_later = (block_ids[:, None] > block_ids[None, :]).astype(F32)
    beyond = jnp.einsum("hqn,nm->hqm", jnp.sum(blocks, axis=-1), block_later)
    suffix = (inside_sum + beyond[..., None]).reshape(heads_here, query_count, key_count)
    weight = jnp.where(causal_mask[None], jnp.exp(jax.nn.log_sigmoid(scores) + suffix), 0.0).astype(
        BF16
    )
    partial_value = jnp.einsum("hqk,khd->qhd", weight, value_heads, preferred_element_type=F32)
    return (partial_value.reshape(query_count, heads_here * HD), jnp.sum(log_remain, axis=-1))


def on_device(tokens, norm_gain, w_query, w_key, w_value, w_out, key_rate):
    tokens_f = tokens.astype(F32)
    normed = (
        tokens_f
        * lax.rsqrt(jnp.mean(tokens_f * tokens_f, axis=-1, keepdims=True) + EPS)
        * norm_gain
    ).astype(BF16)
    queries = jnp.dot(normed, w_query, preferred_element_type=F32).astype(BF16)
    key_rows = jnp.dot(normed, w_key, preferred_element_type=F32).astype(BF16)
    value_rows = jnp.dot(normed, w_value, preferred_element_type=F32).astype(BF16)
    head_width = w_query.shape[1]
    heads_local = head_width // HD
    row_count = tokens.shape[0]
    rate_row_values = jnp.transpose(key_rate)
    query_heads = queries.reshape(row_count, heads_local, HD)
    own_shard = lax.axis_index("sp")
    shard_total = lax.axis_size("sp")
    local_pos = jnp.arange(row_count, dtype=jnp.int32)
    shard_ids = jnp.arange(shard_total, dtype=jnp.int32)
    later_mask = (shard_ids[:, None] > shard_ids[None, :]).astype(F32)
    query_groups = [(query_heads, own_shard * row_count)]

    def summarize(key_block, value_block, rate_block, first_key):
        key_pos = first_key + local_pos
        group_heads, group_start = query_groups[0]
        group_count = group_heads.shape[0]
        group_pos = group_start + jnp.arange(group_count, dtype=jnp.int32)
        empty_pair = (
            jnp.zeros((group_count, head_width), F32),
            jnp.zeros((heads_local, group_count), F32),
        )
        partial_value, remain = lax.cond(
            first_key < group_start + group_count - 1,
            lambda: shard_summary(
                group_heads, key_block, value_block, rate_block, group_pos, key_pos
            ),
            lambda: empty_pair,
        )
        partial_list = [partial_value]
        remain_list = [remain]
        return (jnp.concatenate(partial_list, axis=0), jnp.concatenate(remain_list, axis=1))

    initial = (
        jnp.zeros((shard_total, row_count, head_width), F32),
        jnp.zeros((shard_total, heads_local, row_count), F32),
    )
    piece_keys, piece_values, piece_rates = sent_together(
        (key_rows, value_rows, rate_row_values), "sp", 0, 1
    )
    piece_count = piece_keys.shape[0] // row_count
    key_blocks = piece_keys.reshape(piece_count, row_count, heads_local, HD)
    value_blocks = piece_values.reshape(piece_count, row_count, heads_local, HD)
    rate_blocks = piece_rates.reshape(piece_count, row_count, heads_local)

    def absorb_one(inner_pair, item_tuple):
        item_index, key_block, value_block, rate_block = item_tuple
        first_key = item_index * row_count
        shard_index = first_key // row_count
        partial_value, remain = summarize(key_block, value_block, rate_block, first_key)
        partials = lax.dynamic_update_index_in_dim(inner_pair[0], partial_value, shard_index, 0)
        remains = lax.dynamic_update_index_in_dim(inner_pair[1], remain, shard_index, 0)
        return ((partials, remains), None)

    result, _ = lax.scan(
        absorb_one,
        initial,
        (jnp.arange(piece_count, dtype=jnp.int32), key_blocks, value_blocks, rate_blocks),
    )
    partials, remains = result
    beyond = jnp.einsum("nhq,nm->mhq", remains, later_mask)
    factor = jnp.transpose(jnp.exp(beyond), (0, 2, 1))[..., None]
    mixed_rows = jnp.sum(partials.reshape(shard_total, row_count, heads_local, HD) * factor, axis=0)
    mixed = mixed_rows.reshape(row_count, head_width).astype(BF16)
    token_heads = lax.all_to_all(mixed, "tp", split_axis=0, concat_axis=1, tiled=True)
    whole_out = lax.all_gather(w_out, "tp", axis=0, tiled=True)
    own_rows = jnp.dot(token_heads, whole_out, preferred_element_type=F32).astype(BF16)
    return gather_directly(own_rows, "tp", 0)


def solution(mesh):
    return jax.shard_map(
        on_device,
        mesh=mesh,
        in_specs=(
            P(("grp", "sp"), None),
            P(),
            P(None, "tp"),
            P(None, "tp"),
            P(None, "tp"),
            P("tp", None),
            P("tp", ("grp", "sp")),
        ),
        out_specs=P(("grp", "sp"), None),
        check_vma=False,
    )
```

profile of v0, /device:TPU:2016, one launch (start us, length us, event | category | flops | bytes accessed | tf_op | source)
XLA Modules:
  0.0 354.9 jit_solution(2087388215838886305)
XLA Ops:
  13.0 122.8 %all-gather.3.cloned.1.call-done = bf16[4096,258]{0,1:T(8,128)(2,1)} async-done(((bf16[128,258]{0,1:T(8,128)(2,1)}), bf16[4096,258]{0,1:T(8,128)(2,1)}) %all-gather.3.cloned.1.call-update) | async-done | bytes 2113552 | tf_op jit(solution)/shard_map/all_gather | solution.py:21
  142.0 179.5 %while.16 = (s32[]{:T(128)}, f32[32,128,128]{1,2,0:T(8,128)S(1)}, bf16[32,2,128]{2,0,1:T(8,128)(2,1)S(1)}, s32[32]{0:T(128)S(1)}, s32[]{:T(128)}, /*index=5*/s32...) while((s32[]{:T(128)}, f32[32,128,128]{1,2,0:T(8,128)S(1)}, ...), condition=%wide.region_5.6_spmd.clone, body=%wide.region_1.5_spmd.clone.sunk | while | flops 17826308 | bytes 767463 | solution.py:136
  143.3 3.6 %conditional.3 = (f32[1,128,128]{1,2,0:T(8,128)S(1)}, f32[1,2,128]{2,1,0:T(2,128)}) conditional(s32[]{:T(128)} %convert_element_type.84, () %tuple.62, (s32[]{:T(128)}, s32[128]{0:T(128)S(1)}, s32[]{:T(128)}, s32[128]{0:T(128)S(1)}, bf16[32,128,2,64]{1,3,2,0:T(8,128)(2,1)}, /*index=5*/s32[]{:T(128)}, bf16[128,2,64]{0,2,1:T(8,128)(2,1)S(1)}, ...), branch_computations={%region_2.2_spmd, %region_3.4_spmd} | conditional | flops 17826304 | bytes 633372 | solution.py:104
  148.9 3.6 %conditional.3 = (f32[1,128,128]{1,2,0:T(8,128)S(1)}, f32[1,2,128]{2,1,0:T(2,128)}) conditional(s32[]{:T(128)} %convert_element_type.84, () %tuple.62, (s32[]{:T(128)}, s32[128]{0:T(128)S(1)}, s32[]{:T(128)}, s32[128]{0:T(128)S(1)}, bf16[32,128,2,64]{1,3,2,0:T(8,128)(2,1)}, /*index=5*/s32[]{:T(128)}, bf16[128,2,64]{0,2,1:T(8,128)(2,1)S(1)}, ...), branch_computations={%region_2.2_spmd, %region_3.4_spmd} | conditional | flops 17826304 | bytes 633372 | solution.py:104
  154.5 3.6 %conditional.3 = (f32[1,128,128]{1,2,0:T(8,128)S(1)}, f32[1,2,128]{2,1,0:T(2,128)}) conditional(s32[]{:T(128)} %convert_element_type.84, () %tuple.62, (s32[]{:T(128)}, s32[128]{0:T(128)S(1)}, s32[]{:T(128)}, s32[128]{0:T(128)S(1)}, bf16[32,128,2,64]{1,3,2,0:T(8,128)(2,1)}, /*index=5*/s32[]{:T(128)}, bf16[128,2,64]{0,2,1:T(8,128)(2,1)S(1)}, ...), branch_computations={%region_2.2_spmd, %region_3.4_spmd} | conditional | flops 17826304 | bytes 633372 | solution.py:104
  160.1 3.6 %conditional.3 = (f32[1,128,128]{1,2,0:T(8,128)S(1)}, f32[1,2,128]{2,1,0:T(2,128)}) conditional(s32[]{:T(128)} %convert_element_type.84, () %tuple.62, (s32[]{:T(128)}, s32[128]{0:T(128)S(1)}, s32[]{:T(128)}, s32[128]{0:T(128)S(1)}, bf16[32,128,2,64]{1,3,2,0:T(8,128)(2,1)}, /*index=5*/s32[]{:T(128)}, bf16[128,2,64]{0,2,1:T(8,128)(2,1)S(1)}, ...), branch_computations={%region_2.2_spmd, %region_3.4_spmd} | conditional | flops 17826304 | bytes 633372 | solution.py:104
  165.7 3.6 %conditional.3 = (f32[1,128,128]{1,2,0:T(8,128)S(1)}, f32[1,2,128]{2,1,0:T(2,128)}) conditional(s32[]{:T(128)} %convert_element_type.84, () %tuple.62, (s32[]{:T(128)}, s32[128]{0:T(128)S(1)}, s32[]{:T(128)}, s32[128]{0:T(128)S(1)}, bf16[32,128,2,64]{1,3,2,0:T(8,128)(2,1)}, /*index=5*/s32[]{:T(128)}, bf16[128,2,64]{0,2,1:T(8,128)(2,1)S(1)}, ...), branch_computations={%region_2.2_spmd, %region_3.4_spmd} | conditional | flops 17826304 | bytes 633372 | solution.py:104
  171.3 3.6 %conditional.3 = (f32[1,128,128]{1,2,0:T(8,128)S(1)}, f32[1,2,128]{2,1,0:T(2,128)}) conditional(s32[]{:T(128)} %convert_element_type.84, () %tuple.62, (s32[]{:T(128)}, s32[128]{0:T(128)S(1)}, s32[]{:T(128)}, s32[128]{0:T(128)S(1)}, bf16[32,128,2,64]{1,3,2,0:T(8,128)(2,1)}, /*index=5*/s32[]{:T(128)}, bf16[128,2,64]{0,2,1:T(8,128)(2,1)S(1)}, ...), branch_computations={%region_2.2_spmd, %region_3.4_spmd} | conditional | flops 17826304 | bytes 633372 | solution.py:104
  176.9 3.6 %conditional.3 = (f32[1,128,128]{1,2,0:T(8,128)S(1)}, f32[1,2,128]{2,1,0:T(2,128)}) conditional(s32[]{:T(128)} %convert_element_type.84, () %tuple.62, (s32[]{:T(128)}, s32[128]{0:T(128)S(1)}, s32[]{:T(128)}, s32[128]{0:T(128)S(1)}, bf16[32,128,2,64]{1,3,2,0:T(8,128)(2,1)}, /*index=5*/s32[]{:T(128)}, bf16[128,2,64]{0,2,1:T(8,128)(2,1)S(1)}, ...), branch_computations={%region_2.2_spmd, %region_3.4_spmd} | conditional | flops 17826304 | bytes 633372 | solution.py:104
  182.5 3.6 %conditional.3 = (f32[1,128,128]{1,2,0:T(8,128)S(1)}, f32[1,2,128]{2,1,0:T(2,128)}) conditional(s32[]{:T(128)} %convert_element_type.84, () %tuple.62, (s32[]{:T(128)}, s32[128]{0:T(128)S(1)}, s32[]{:T(128)}, s32[128]{0:T(128)S(1)}, bf16[32,128,2,64]{1,3,2,0:T(8,128)(2,1)}, /*index=5*/s32[]{:T(128)}, bf16[128,2,64]{0,2,1:T(8,128)(2,1)S(1)}, ...), branch_computations={%region_2.2_spmd, %region_3.4_spmd} | conditional | flops 17826304 | bytes 633372 | solution.py:104
  188.1 3.6 %conditional.3 = (f32[1,128,128]{1,2,0:T(8,128)S(1)}, f32[1,2,128]{2,1,0:T(2,128)}) conditional(s32[]{:T(128)} %convert_element_type.84, () %tuple.62, (s32[]{:T(128)}, s32[128]{0:T(128)S(1)}, s32[]{:T(128)}, s32[128]{0:T(128)S(1)}, bf16[32,128,2,64]{1,3,2,0:T(8,128)(2,1)}, /*index=5*/s32[]{:T(128)}, bf16[128,2,64]{0,2,1:T(8,128)(2,1)S(1)}, ...), branch_computations={%region_2.2_spmd, %region_3.4_spmd} | conditional | flops 17826304 | bytes 633372 | solution.py:104
  193.7 3.6 %conditional.3 = (f32[1,128,128]{1,2,0:T(8,128)S(1)}, f32[1,2,128]{2,1,0:T(2,128)}) conditional(s32[]{:T(128)} %convert_element_type.84, () %tuple.62, (s32[]{:T(128)}, s32[128]{0:T(128)S(1)}, s32[]{:T(128)}, s32[128]{0:T(128)S(1)}, bf16[32,128,2,64]{1,3,2,0:T(8,128)(2,1)}, /*index=5*/s32[]{:T(128)}, bf16[128,2,64]{0,2,1:T(8,128)(2,1)S(1)}, ...), branch_computations={%region_2.2_spmd, %region_3.4_spmd} | conditional | flops 17826304 | bytes 633372 | solution.py:104
  199.4 3.6 %conditional.3 = (f32[1,128,128]{1,2,0:T(8,128)S(1)}, f32[1,2,128]{2,1,0:T(2,128)}) conditional(s32[]{:T(128)} %convert_element_type.84, () %tuple.62, (s32[]{:T(128)}, s32[128]{0:T(128)S(1)}, s32[]{:T(128)}, s32[128]{0:T(128)S(1)}, bf16[32,128,2,64]{1,3,2,0:T(8,128)(2,1)}, /*index=5*/s32[]{:T(128)}, bf16[128,2,64]{0,2,1:T(8,128)(2,1)S(1)}, ...), branch_computations={%region_2.2_spmd, %region_3.4_spmd} | conditional | flops 17826304 | bytes 633372 | solution.py:104
  205.0 3.6 %conditional.3 = (f32[1,128,128]{1,2,0:T(8,128)S(1)}, f32[1,2,128]{2,1,0:T(2,128)}) conditional(s32[]{:T(128)} %convert_element_type.84, () %tuple.62, (s32[]{:T(128)}, s32[128]{0:T(128)S(1)}, s32[]{:T(128)}, s32[128]{0:T(128)S(1)}, bf16[32,128,2,64]{1,3,2,0:T(8,128)(2,1)}, /*index=5*/s32[]{:T(128)}, bf16[128,2,64]{0,2,1:T(8,128)(2,1)S(1)}, ...), branch_computations={%region_2.2_spmd, %region_3.4_spmd} | conditional | flops 17826304 | bytes 633372 | solution.py:104
  210.6 3.6 %conditional.3 = (f32[1,128,128]{1,2,0:T(8,128)S(1)}, f32[1,2,128]{2,1,0:T(2,128)}) conditional(s32[]{:T(128)} %convert_element_type.84, () %tuple.62, (s32[]{:T(128)}, s32[128]{0:T(128)S(1)}, s32[]{:T(128)}, s32[128]{0:T(128)S(1)}, bf16[32,128,2,64]{1,3,2,0:T(8,128)(2,1)}, /*index=5*/s32[]{:T(128)}, bf16[128,2,64]{0,2,1:T(8,128)(2,1)S(1)}, ...), branch_computations={%region_2.2_spmd, %region_3.4_spmd} | conditional | flops 17826304 | bytes 633372 | solution.py:104
  216.2 3.6 %conditional.3 = (f32[1,128,128]{1,2,0:T(8,128)S(1)}, f32[1,2,128]{2,1,0:T(2,128)}) conditional(s32[]{:T(128)} %convert_element_type.84, () %tuple.62, (s32[]{:T(128)}, s32[128]{0:T(128)S(1)}, s32[]{:T(128)}, s32[128]{0:T(128)S(1)}, bf16[32,128,2,64]{1,3,2,0:T(8,128)(2,1)}, /*index=5*/s32[]{:T(128)}, bf16[128,2,64]{0,2,1:T(8,128)(2,1)S(1)}, ...), branch_computations={%region_2.2_spmd, %region_3.4_spmd} | conditional | flops 17826304 | bytes 633372 | solution.py:104
  221.8 3.6 %conditional.3 = (f32[1,128,128]{1,2,0:T(8,128)S(1)}, f32[1,2,128]{2,1,0:T(2,128)}) conditional(s32[]{:T(128)} %convert_element_type.84, () %tuple.62, (s32[]{:T(128)}, s32[128]{0:T(128)S(1)}, s32[]{:T(128)}, s32[128]{0:T(128)S(1)}, bf16[32,128,2,64]{1,3,2,0:T(8,128)(2,1)}, /*index=5*/s32[]{:T(128)}, bf16[128,2,64]{0,2,1:T(8,128)(2,1)S(1)}, ...), branch_computations={%region_2.2_spmd, %region_3.4_spmd} | conditional | flops 17826304 | bytes 633372 | solution.py:104
  227.4 3.6 %conditional.3 = (f32[1,128,128]{1,2,0:T(8,128)S(1)}, f32[1,2,128]{2,1,0:T(2,128)}) conditional(s32[]{:T(128)} %convert_element_type.84, () %tuple.62, (s32[]{:T(128)}, s32[128]{0:T(128)S(1)}, s32[]{:T(128)}, s32[128]{0:T(128)S(1)}, bf16[32,128,2,64]{1,3,2,0:T(8,128)(2,1)}, /*index=5*/s32[]{:T(128)}, bf16[128,2,64]{0,2,1:T(8,128)(2,1)S(1)}, ...), branch_computations={%region_2.2_spmd, %region_3.4_spmd} | conditional | flops 17826304 | bytes 633372 | solution.py:104
  233.0 3.6 %conditional.3 = (f32[1,128,128]{1,2,0:T(8,128)S(1)}, f32[1,2,128]{2,1,0:T(2,128)}) conditional(s32[]{:T(128)} %convert_element_type.84, () %tuple.62, (s32[]{:T(128)}, s32[128]{0:T(128)S(1)}, s32[]{:T(128)}, s32[128]{0:T(128)S(1)}, bf16[32,128,2,64]{1,3,2,0:T(8,128)(2,1)}, /*index=5*/s32[]{:T(128)}, bf16[128,2,64]{0,2,1:T(8,128)(2,1)S(1)}, ...), branch_computations={%region_2.2_spmd, %region_3.4_spmd} | conditional | flops 17826304 | bytes 633372 | solution.py:104
  238.6 3.6 %conditional.3 = (f32[1,128,128]{1,2,0:T(8,128)S(1)}, f32[1,2,128]{2,1,0:T(2,128)}) conditional(s32[]{:T(128)} %convert_element_type.84, () %tuple.62, (s32[]{:T(128)}, s32[128]{0:T(128)S(1)}, s32[]{:T(128)}, s32[128]{0:T(128)S(1)}, bf16[32,128,2,64]{1,3,2,0:T(8,128)(2,1)}, /*index=5*/s32[]{:T(128)}, bf16[128,2,64]{0,2,1:T(8,128)(2,1)S(1)}, ...), branch_computations={%region_2.2_spmd, %region_3.4_spmd} | conditional | flops 17826304 | bytes 633372 | solution.py:104
  244.2 3.6 %conditional.3 = (f32[1,128,128]{1,2,0:T(8,128)S(1)}, f32[1,2,128]{2,1,0:T(2,128)}) conditional(s32[]{:T(128)} %convert_element_type.84, () %tuple.62, (s32[]{:T(128)}, s32[128]{0:T(128)S(1)}, s32[]{:T(128)}, s32[128]{0:T(128)S(1)}, bf16[32,128,2,64]{1,3,2,0:T(8,128)(2,1)}, /*index=5*/s32[]{:T(128)}, bf16[128,2,64]{0,2,1:T(8,128)(2,1)S(1)}, ...), branch_computations={%region_2.2_spmd, %region_3.4_spmd} | conditional | flops 17826304 | bytes 633372 | solution.py:104
  249.8 3.6 %conditional.3 = (f32[1,128,128]{1,2,0:T(8,128)S(1)}, f32[1,2,128]{2,1,0:T(2,128)}) conditional(s32[]{:T(128)} %convert_element_type.84, () %tuple.62, (s32[]{:T(128)}, s32[128]{0:T(128)S(1)}, s32[]{:T(128)}, s32[128]{0:T(128)S(1)}, bf16[32,128,2,64]{1,3,2,0:T(8,128)(2,1)}, /*index=5*/s32[]{:T(128)}, bf16[128,2,64]{0,2,1:T(8,128)(2,1)S(1)}, ...), branch_computations={%region_2.2_spmd, %region_3.4_spmd} | conditional | flops 17826304 | bytes 633372 | solution.py:104
  255.4 3.6 %conditional.3 = (f32[1,128,128]{1,2,0:T(8,128)S(1)}, f32[1,2,128]{2,1,0:T(2,128)}) conditional(s32[]{:T(128)} %convert_element_type.84, () %tuple.62, (s32[]{:T(128)}, s32[128]{0:T(128)S(1)}, s32[]{:T(128)}, s32[128]{0:T(128)S(1)}, bf16[32,128,2,64]{1,3,2,0:T(8,128)(2,1)}, /*index=5*/s32[]{:T(128)}, bf16[128,2,64]{0,2,1:T(8,128)(2,1)S(1)}, ...), branch_computations={%region_2.2_spmd, %region_3.4_spmd} | conditional | flops 17826304 | bytes 633372 | solution.py:104
  261.0 3.6 %conditional.3 = (f32[1,128,128]{1,2,0:T(8,128)S(1)}, f32[1,2,128]{2,1,0:T(2,128)}) conditional(s32[]{:T(128)} %convert_element_type.84, () %tuple.62, (s32[]{:T(128)}, s32[128]{0:T(128)S(1)}, s32[]{:T(128)}, s32[128]{0:T(128)S(1)}, bf16[32,128,2,64]{1,3,2,0:T(8,128)(2,1)}, /*index=5*/s32[]{:T(128)}, bf16[128,2,64]{0,2,1:T(8,128)(2,1)S(1)}, ...), branch_computations={%region_2.2_spmd, %region_3.4_spmd} | conditional | flops 17826304 | bytes 633372 | solution.py:104
  266.6 3.6 %conditional.3 = (f32[1,128,128]{1,2,0:T(8,128)S(1)}, f32[1,2,128]{2,1,0:T(2,128)}) conditional(s32[]{:T(128)} %convert_element_type.84, () %tuple.62, (s32[]{:T(128)}, s32[128]{0:T(128)S(1)}, s32[]{:T(128)}, s32[128]{0:T(128)S(1)}, bf16[32,128,2,64]{1,3,2,0:T(8,128)(2,1)}, /*index=5*/s32[]{:T(128)}, bf16[128,2,64]{0,2,1:T(8,128)(2,1)S(1)}, ...), branch_computations={%region_2.2_spmd, %region_3.4_spmd} | conditional | flops 17826304 | bytes 633372 | solution.py:104
  272.2 3.6 %conditional.3 = (f32[1,128,128]{1,2,0:T(8,128)S(1)}, f32[1,2,128]{2,1,0:T(2,128)}) conditional(s32[]{:T(128)} %convert_element_type.84, () %tuple.62, (s32[]{:T(128)}, s32[128]{0:T(128)S(1)}, s32[]{:T(128)}, s32[128]{0:T(128)S(1)}, bf16[32,128,2,64]{1,3,2,0:T(8,128)(2,1)}, /*index=5*/s32[]{:T(128)}, bf16[128,2,64]{0,2,1:T(8,128)(2,1)S(1)}, ...), branch_computations={%region_2.2_spmd, %region_3.4_spmd} | conditional | flops 17826304 | bytes 633372 | solution.py:104
  277.9 3.6 %conditional.3 = (f32[1,128,128]{1,2,0:T(8,128)S(1)}, f32[1,2,128]{2,1,0:T(2,128)}) conditional(s32[]{:T(128)} %convert_element_type.84, () %tuple.62, (s32[]{:T(128)}, s32[128]{0:T(128)S(1)}, s32[]{:T(128)}, s32[128]{0:T(128)S(1)}, bf16[32,128,2,64]{1,3,2,0:T(8,128)(2,1)}, /*index=5*/s32[]{:T(128)}, bf16[128,2,64]{0,2,1:T(8,128)(2,1)S(1)}, ...), branch_computations={%region_2.2_spmd, %region_3.4_spmd} | conditional | flops 17826304 | bytes 633372 | solution.py:104
  283.5 3.6 %conditional.3 = (f32[1,128,128]{1,2,0:T(8,128)S(1)}, f32[1,2,128]{2,1,0:T(2,128)}) conditional(s32[]{:T(128)} %convert_element_type.84, () %tuple.62, (s32[]{:T(128)}, s32[128]{0:T(128)S(1)}, s32[]{:T(128)}, s32[128]{0:T(128)S(1)}, bf16[32,128,2,64]{1,3,2,0:T(8,128)(2,1)}, /*index=5*/s32[]{:T(128)}, bf16[128,2,64]{0,2,1:T(8,128)(2,1)S(1)}, ...), branch_computations={%region_2.2_spmd, %region_3.4_spmd} | conditional | flops 17826304 | bytes 633372 | solution.py:104
  300.3 3.6 %conditional.3 = (f32[1,128,128]{1,2,0:T(8,128)S(1)}, f32[1,2,128]{2,1,0:T(2,128)}) conditional(s32[]{:T(128)} %convert_element_type.84, () %tuple.62, (s32[]{:T(128)}, s32[128]{0:T(128)S(1)}, s32[]{:T(128)}, s32[128]{0:T(128)S(1)}, bf16[32,128,2,64]{1,3,2,0:T(8,128)(2,1)}, /*index=5*/s32[]{:T(128)}, bf16[128,2,64]{0,2,1:T(8,128)(2,1)S(1)}, ...), branch_computations={%region_2.2_spmd, %region_3.4_spmd} | conditional | flops 17826304 | bytes 633372 | solution.py:104
  311.5 3.6 %conditional.3 = (f32[1,128,128]{1,2,0:T(8,128)S(1)}, f32[1,2,128]{2,1,0:T(2,128)}) conditional(s32[]{:T(128)} %convert_element_type.84, () %tuple.62, (s32[]{:T(128)}, s32[128]{0:T(128)S(1)}, s32[]{:T(128)}, s32[128]{0:T(128)S(1)}, bf16[32,128,2,64]{1,3,2,0:T(8,128)(2,1)}, /*index=5*/s32[]{:T(128)}, bf16[128,2,64]{0,2,1:T(8,128)(2,1)S(1)}, ...), branch_computations={%region_2.2_spmd, %region_3.4_spmd} | conditional | flops 17826304 | bytes 633372 | solution.py:104
  322.0 9.5 %all_to_all.21 = bf16[8,16,128]{2,1,0:T(8,128)(2,1)S(1)} all-to-all(bf16[8,16,128]{2,1,0:T(8,128)(2,1)S(1)} %bitcast.76), channel_id=1, replica_groups=mesh['grp'=2,'sp'=32,'tp'=8] {'tp'}, dimensions={0} | all-to-all | bytes 65536 | tf_op jit(solution)/shard_map/all_to_all | solution.py:146
  334.4 12.8 %all_to_all.22 = bf16[8,16,2048]{2,1,0:T(8,128)(2,1)S(1)} all-to-all(bf16[8,16,2048]{2,1,0:T(8,128)(2,1)S(1)} %broadcast_in_dim.66), channel_id=1, replica_groups=mesh['grp'=2,'sp'=32,'tp'=8] {'tp'}, dimensions={0} | all-to-all | bytes 1048576 | tf_op jit(solution)/shard_map/all_to_all | solution.py:26
  (361 shorter events, 186.5 us)
Async XLA Ops:
  6.5 1.4 copy-start
  6.6 6.0 %copy-start.1 = (bf16[128,2048]{1,0:T(8,128)(2,1)S(1)}, bf16[128,2048]{1,0:T(8,128)(2,1)}, u32[]{:S(2)}) copy-start(bf16[128,2048]{1,0:T(8,128)(2,1)} %param.11) | copy-start | bytes 1572868
  6.6 6.0 %copy-start.4 = (f32[2048]{0:T(1024)S(1)}, f32[2048]{0:T(1024)}, u32[]{:S(2)}) copy-start(f32[2048]{0:T(1024)} %param.12) | copy-start | bytes 24580
  6.6 4.5 %copy-start.2 = (bf16[2,128]{1,0:T(2,128)(2,1)S(1)}, bf16[2,128]{1,0:T(2,128)(2,1)}, u32[]{:S(2)}) copy-start(bf16[2,128]{1,0:T(2,128)(2,1)} %param.17) | copy-start | bytes 1540
  6.6 6.0 %copy-start.3 = (bf16[2048,128]{1,0:T(8,128)(2,1)S(1)}, bf16[2048,128]{1,0:T(8,128)(2,1)}, u32[]{:S(2)}) copy-start(bf16[2048,128]{1,0:T(8,128)(2,1)} %param.13) | copy-start | bytes 1572868
  6.6 129.3 %all-gather.3.cloned.1.call-start = ((), (), s32[]{:S(2)}) async-start(), calls=%async_computation.2 | async-start | bytes 2230272 | tf_op jit(solution)/shard_map/all_gather | solution.py:21
  11.8 319.7 %all-gather.5.cloned.1.call-start = ((), (), s32[]{:S(2)}) async-start(), calls=%async_computation.3 | async-start | bytes 4718592 | tf_op jit(solution)/shard_map/all_gather | solution.py:147
Sparse Core Ops, SparseCore 0:
  11.9 123.9 all-gather.2
  138.0 42.3 all-gather.4
where the time goes:
time: 361 us; the launch traced here: 355 us
  waiting for transfers between devices  124 us (34%)
  matrix products  95 us (26%)
  local copies, waits for them, and re-layouts  48.9 us (14%)
  other arithmetic  27.2 us (8%)
  loops' own time  24 us (7%)
  blocking collectives  22.4 us (6%)
  between operations  13.6 us (4%)
    all_gather x1, waiting for transfers between devices, sent_together(): lax.all_gather(both, axis, axis=dim, tiled=True)  123 us
    dot_general x32, matrix products, break_scores(): jnp.einsum('qhd,khd->hqk', query_heads, key_heads, preferred_element_type...  52.3 us
    dot_general x32, matrix products, shard_summary(): jnp.einsum('hqk,khd->qhd', weight, value_heads, preferred_element_type=F32)  36.4 us
    dynamic_update_slice x32, local copies, waits for them, and re-layouts, absorb_one(): lax.dynamic_update_index_in_dim(inner_pair[1], remain, shard_index, 0)  22.7 us
    another operation x1, loops' own time, on_device(): lax.scan(absorb_one, initial, (jnp.arange(piece_count, dtype=jnp.int32),...  22.6 us
    dot_general x32, other arithmetic, shard_summary(): beyond = jnp.einsum('hqn,nm->hqm', jnp.sum(blocks, axis=-1), block_later)  21.8 us
    dynamic_slice x32, local copies, waits for them, and re-layouts, on_device(): lax.scan(absorb_one, initial, (jnp.arange(piece_count, dtype=jnp.int32),...  18.6 us
    all_to_all x1, blocking collectives, from_everyone(): lax.all_to_all(jnp.broadcast_to(shard[None], (count, *shard.shape)), axis...  12.8 us
  transfers between devices with their start and end apart: 2, of which 1 were waited for; matrix products, arithmetic and copies ran while one was open for 46% of the time, Pallas kernels for 0%

commit v1 on v0

v1 whole, which is shorter than its diff:
```python
import functools

import jax
import jax.numpy as jnp
from jax import lax
from jax.experimental import pallas as pl
from jax.experimental.pallas import tpu as pltpu
from jax.sharding import PartitionSpec as P

HD = 64
SPAN = 128
PAD = 16

F32 = jnp.float32
BF16 = jnp.bfloat16
EPS = 1e-06
MESH = pl.DeviceIdType.MESH


def dot(a, b):
    return lax.dot_general(a, b, (((1,), (0,)), ((), ())), preferred_element_type=F32)


def dot_t(a, b):
    return lax.dot_general(a, b, (((1,), (1,)), ((), ())), preferred_element_type=F32)


def layer(
    nsp,
    ntp,
    far,
    tokens,
    gain,
    w_query,
    w_key,
    w_value,
    w_out,
    rate,
    out,
    kv,
    normed,
    other_tokens,
    queries,
    first_queries,
    far_sent,
    far_in,
    far_queries,
    far_back,
    far_got,
    tri,
    rate_now,
    late_rate,
    acc,
    past,
    mixed,
    first_mixed,
    w_all,
    total,
    late_sem,
    kv_send,
    kv_recv,
    w_send,
    w_recv,
    mx_send,
    mx_recv,
    tok_send,
    tok_recv,
    lr_send,
    lr_recv,
    fq_send,
    fq_recv,
    fa_send,
    fa_recv,
):
    z = lax.axis_index("sp")
    t = lax.axis_index("tp")
    chips = ntp // 2
    x, core = t // 2, lax.rem(t, 2)
    sibling = 2 * x + 1 - core
    reach = nsp - 1 - far
    lead = t == 0
    first = z == 0
    last = z == nsp - 1
    outset = jnp.logical_and(first, lead)
    deputy = jnp.logical_and(z == 1, lead)
    helper = jnp.logical_and(first, t == 1)
    host = jnp.logical_and(z >= 1, z <= reach)
    guest = z > far

    bar = pltpu.get_barrier_semaphore()

    def at(zz, tt):
        return {"sp": zz, "tp": tt}

    def greet(zz, tt):
        pl.semaphore_signal(bar, inc=1, device_id=at(zz, tt), device_id_type=MESH)

    def send(src, dst, ss, rs, zz, tt):
        return pltpu.make_async_remote_copy(
            src_ref=src, dst_ref=dst, send_sem=ss, recv_sem=rs, device_id=at(zz, tt), device_id_type=MESH
        )

    @pl.when(z >= 1)
    def _():
        greet(z - 1, t)

    for p in range(ntp):

        @pl.when(jnp.logical_and(t != 0, t != p))
        def _():
            greet(z, p)

    @pl.when(host)
    def _():
        greet(z + far, t)

    @pl.when(jnp.logical_and(jnp.logical_and(host, lead), z >= 2))
    def _():
        greet(0, 0)

    @pl.when(jnp.logical_and(first, t != 0))
    def _():
        greet(1, 0)

    @pl.when(deputy)
    def _():
        greet(0, 1)

    one = lambda flag: jnp.where(flag, 1, 0)
    expected = (
        one(jnp.logical_not(last))
        + jnp.where(lead, ntp - 1, ntp - 2)
        + one(guest)
        + one(outset) * (reach - 1)
        + one(deputy) * (ntp - 1)
        + one(helper)
    )

    row = lax.broadcasted_iota(jnp.int32, (2 * SPAN, 2 * SPAN), 0)
    col = lax.broadcasted_iota(jnp.int32, (2 * SPAN, 2 * SPAN), 1)
    later = jnp.logical_or(col >= SPAN, lax.rem(row, SPAN) >= col)
    tri[...] = jnp.where(later, 1.0, 0.0).astype(BF16)

    def split_heads(dst, q):
        lane = lax.broadcasted_iota(jnp.int32, (SPAN, 2 * HD), 1)
        qf = q.astype(F32)
        dst[:SPAN] = jnp.where(lane < HD, qf, 0.0).astype(BF16)
        dst[SPAN:] = jnp.where(lane >= HD, qf, 0.0).astype(BF16)

    def join_heads(a):
        lane = lax.broadcasted_iota(jnp.int32, (SPAN, 2 * HD), 1)
        return jnp.where(lane < HD, a[:SPAN], a[SPAN:])

    def project(src, slot):
        xs = src[...].astype(F32)
        scale = lax.rsqrt(jnp.mean(xs * xs, axis=-1, keepdims=True) + EPS)
        normed[...] = (xs * scale * gain[...]).astype(BF16)
        kv[slot, pl.ds(0, SPAN)] = dot(normed[...], w_key[...]).astype(BF16)
        kv[slot, pl.ds(SPAN, SPAN)] = dot(normed[...], w_value[...]).astype(BF16)
        kv[slot, pl.ds(2 * SPAN, PAD)] = jnp.concatenate(
            [rate[...].astype(F32), jnp.zeros((PAD - 2, SPAN), F32)], axis=0
        ).astype(BF16)
        return dot(normed[...], w_query[...]).astype(BF16) * HD ** (-0.5)

    def attend(q_ref, slot, diagonal):
        s = dot_t(q_ref[...], kv[slot, pl.ds(0, SPAN)])
        s = jnp.concatenate([s[:SPAN] + rate_now[0:1], s[SPAN:] + rate_now[1:2]], axis=0)
        soft = jnp.maximum(s, 0.0) + jnp.log(1.0 + jnp.exp(-jnp.abs(s)))
        if diagonal:
            r = lax.rem(lax.broadcasted_iota(jnp.int32, (2 * SPAN, SPAN), 0), SPAN)
            c = lax.broadcasted_iota(jnp.int32, (2 * SPAN, SPAN), 1)
            seen = c < r
            soft = jnp.where(seen, soft, 0.0)
        high = soft.astype(BF16)
        low = (soft - high.astype(F32)).astype(BF16)
        sums = dot(jnp.concatenate([high, low], axis=1), tri[...])
        weight = jnp.exp(s - sums[:, :SPAN])
        if diagonal:
            weight = jnp.where(seen, weight, 0.0)
        part = dot(weight.astype(BF16), kv[slot, pl.ds(SPAN, SPAN)])
        if diagonal:
            acc[...] = part
            past[...] = sums[:, SPAN:]
        else:
            acc[...] = acc[...] + jnp.exp(-past[...]) * part
            past[...] = past[...] + sums[:, SPAN:]

    def slab_rate(slot):
        rate_now[...] = kv[slot, pl.ds(2 * SPAN, PAD)][:2].astype(F32)

    @pl.when(jnp.logical_not(outset))
    def _():
        q = project(tokens, 0)
        far_sent[...] = q
        split_heads(queries, q)
        slab_rate(0)

    pl.semaphore_wait(bar, expected)

    late_rates = [
        send(rate, late_rate, lr_send.at[i - 1], lr_recv, i, 0) for i in range(1, reach + 1)
    ]
    borrowed = send(tokens, other_tokens, tok_send, tok_recv, 1, 0)

    def w_copy(src, slot, sem, zz, tt):
        return send(src, w_all.at[slot], w_send.at[sem], w_recv.at[slot], zz, tt)

    def across(d):
        return 2 * lax.rem(x + d, chips) + core

    directs = [w_copy(w_out, t, d - 1, z, across(d)) for d in range(1, chips)]
    to_sibling = w_copy(w_out, t, chips - 1, z, sibling)
    passed = [w_copy(w_all.at[across(d)], across(d), chips - 1 + d, z, sibling) for d in range(1, chips)]
    lent = [w_copy(w_out, 0, 2 * chips - 1 + i, 0, p) for i, p in enumerate([1] + list(range(2, ntp, 2)))]
    to_helper = w_copy(w_out, t, 3 * chips - 1, 0, 1)

    def kv_copy(k):
        return send(kv.at[k], kv.at[k + 1], kv_send.at[k], kv_recv.at[k + 1], z + 1, t)

    def mx_copy(p):
        return send(mixed.at[t], mixed.at[t], mx_send.at[p], mx_recv.at[t], z, p)

    def first_copy(p):
        return send(first_mixed, mixed.at[0], mx_send.at[ntp + p], mx_recv.at[0], 0, p)

    ask = send(far_sent, far_in, fq_send, fq_recv, z - far, t)
    answer = send(far_back, far_got, fa_send, fa_recv, z + far, t)

    received = jnp.where(z <= reach, z, far)
    forwarded = jnp.where(last, 0, jnp.where(z + 1 <= reach, z + 1, far))

    @pl.when(outset)
    def _():
        for c in late_rates:
            c.start()

    @pl.when(helper)
    def _():
        borrowed.start()

    @pl.when(jnp.logical_and(jnp.logical_not(outset), forwarded > 0))
    def _():
        kv_copy(0).start()

    @pl.when(guest)
    def _():
        ask.start()

    @pl.when(lead)
    def _():
        for p in range(1, ntp):
            pl.semaphore_signal(late_sem, inc=1, device_id=at(z, p), device_id_type=MESH)

    @pl.when(jnp.logical_not(outset))
    def _():
        for d in range(1, chips):

            @pl.when(across(d) != 0)
            def _():
                directs[d - 1].start()

        @pl.when(sibling != 0)
        def _():
            to_sibling.start()

    @pl.when(deputy)
    def _():
        for c in lent:
            c.start()

    @pl.when(jnp.logical_and(first, jnp.logical_and(core == 0, t != 0)))
    def _():
        to_helper.start()

    def to_lead():
        pl.semaphore_wait(late_sem, 1)
        for d in range(1, chips):

            @pl.when(across(d) == 0)
            def _():
                directs[d - 1].start()

        @pl.when(sibling == 0)
        def _():
            to_sibling.start()

    @pl.when(jnp.logical_and(z > 0, t != 0))
    def _():
        to_lead()

    w_all[t] = w_out[...]

    @pl.when(deputy)
    def _():
        borrowed.wait_recv()
        q = project(other_tokens, 1)
        split_heads(first_queries, q)
        kv_copy(1).start()

    @pl.when(jnp.logical_not(outset))
    def _():
        attend(queries, 0, True)

    def absorb(k, carry):
        @pl.when(jnp.logical_not(deputy))
        def _():
            kv_copy(k - 1).wait_recv()

            @pl.when(k < forwarded)
            def _():
                kv_copy(k).start()

        reaches_first = jnp.logical_and(lead, k == z)

        @pl.when(reaches_first)
        def _():
            late_rates[0].wait_recv()
            rate_now[...] = late_rate[...].astype(F32)

        @pl.when(jnp.logical_not(reaches_first))
        def _():
            slab_rate(k)

        @pl.when(k <= far)
        def _():
            attend(queries, k, False)

        return carry

    lax.fori_loop(1, received + 1, absorb, 0)

    @pl.when(guest)
    def _():
        answer.wait_recv()
        acc[...] = acc[...] + jnp.exp(-past[...]) * jnp.concatenate([far_got[...].astype(F32)] * 2, axis=0)

    @pl.when(jnp.logical_not(outset))
    def _():
        mixed[t] = join_heads(acc[...]).astype(BF16)

    @pl.when(deputy)
    def _():
        rate_now[...] = late_rate[...].astype(F32)
        attend(first_queries, 1, True)
        first_mixed[...] = join_heads(acc[...]).astype(BF16)
        for p in range(ntp):
            first_copy(p).start()

    @pl.when(jnp.logical_not(outset))
    def _():
        for p in range(1, ntp):

            @pl.when(t != p)
            def _():
                mx_copy(p).start()

    @pl.when(jnp.logical_and(z > 0, t != 0))
    def _():
        mx_copy(0).start()

    for d in range(1, chips):

        @pl.when(jnp.logical_not(outset))
        def _():
            w_copy(w_out, across(d), 0, z, t).wait_recv()

        @pl.when(jnp.logical_not(jnp.logical_and(first, x == 0)))
        def _():
            passed[d - 1].start()

    @pl.when(host)
    def _():
        ask.wait_recv()
        split_heads(far_queries, far_in[...])
        acc[...] = jnp.zeros_like(acc)
        past[...] = jnp.zeros_like(past)

        def absorb_far(k, carry):
            reaches_first = jnp.logical_and(lead, k == z)

            @pl.when(reaches_first)
            def _():
                rate_now[...] = late_rate[...].astype(F32)

            @pl.when(jnp.logical_not(reaches_first))
            def _():
                slab_rate(k)

            attend(far_queries, k, False)
            return carry

        lax.fori_loop(1, z + 1, absorb_far, 0)
        far_back[...] = join_heads(acc[...]).astype(BF16)
        answer.start()

    @pl.when(jnp.logical_and(first, t != 0))
    def _():
        to_lead()
        mx_copy(0).start()

    @pl.when(helper)
    def _():
        for d in range(1, chips):
            passed[d - 1].start()

    def wait_w(slot):
        w_copy(w_out, slot, 0, z, t).wait_recv()

    def wait_mixed(slot):
        send(mixed.at[slot], mixed.at[slot], mx_send.at[0], mx_recv.at[slot], z, t).wait_recv()

    for d in range(chips):
        xx = lax.rem(x + d, chips)
        for c in range(2):
            slot = 2 * xx + c
            same = core == c
            own = jnp.logical_and(d == 0, same)
            pl.when(jnp.logical_or(jnp.logical_not(same), jnp.logical_and(outset, d > 0)))(
                functools.partial(wait_w, slot)
            )
            pl.when(jnp.logical_or(jnp.logical_not(own), outset))(functools.partial(wait_mixed, slot))
        pair = jnp.concatenate([mixed[2 * xx], mixed[2 * xx + 1]], axis=1)
        rows = jnp.concatenate([w_all[2 * xx], w_all[2 * xx + 1]], axis=0)
        part = dot(pair, rows)
        if d == 0:
            total[...] = part
        elif d < chips - 1:
            total[...] = total[...] + part
        else:
            out[...] = (total[...] + part).astype(BF16)
    if chips == 1:
        out[...] = total[...].astype(BF16)

    @pl.when(outset)
    def _():
        for c in late_rates:
            c.wait_send()

    @pl.when(helper)
    def _():
        borrowed.wait_send()

    def sent(k, carry):
        kv_copy(k).wait_send()
        return carry

    @pl.when(jnp.logical_not(outset))
    def _():
        lax.fori_loop(0, forwarded, sent, 0)
        for c in directs:
            c.wait_send()
        to_sibling.wait_send()
        for p in range(ntp):

            @pl.when(t != p)
            def _():
                mx_copy(p).wait_send()

    @pl.when(jnp.logical_or(jnp.logical_not(jnp.logical_and(first, x == 0)), helper))
    def _():
        for c in passed:
            c.wait_send()

    @pl.when(deputy)
    def _():
        for c in lent:
            c.wait_send()
        for p in range(ntp):
            first_copy(p).wait_send()

    @pl.when(jnp.logical_and(first, jnp.logical_and(core == 0, t != 0)))
    def _():
        to_helper.wait_send()

    @pl.when(guest)
    def _():
        ask.wait_send()

    @pl.when(host)
    def _():
        answer.wait_send()


def on_device(tokens, norm_gain, w_query, w_key, w_value, w_out, key_rate):
    nsp, ntp = lax.axis_size("sp"), lax.axis_size("tp")
    rows, d = tokens.shape
    width = w_query.shape[1]
    far = nsp // 2 - 1
    chips = ntp // 2
    dma = pltpu.SemaphoreType.DMA
    vmem = pltpu.VMEM
    return pl.pallas_call(
        functools.partial(layer, nsp, ntp, far),
        out_shape=jax.ShapeDtypeStruct((rows, d), BF16),
        in_specs=[pl.BlockSpec(memory_space=pltpu.VMEM)] * 7,
        out_specs=pl.BlockSpec(memory_space=pltpu.VMEM),
        scratch_shapes=[
            vmem((nsp - far + 1, 2 * SPAN + PAD, width), BF16),
            vmem((rows, d), BF16),
            vmem((rows, d), BF16),
            vmem((2 * rows, width), BF16),
            vmem((2 * rows, width), BF16),
            vmem((rows, width), BF16),
            vmem((rows, width), BF16),
            vmem((2 * rows, width), BF16),
            vmem((rows, width), BF16),
            vmem((rows, width), BF16),
            vmem((2 * SPAN, 2 * SPAN), BF16),
            vmem((2, SPAN), F32),
            vmem((2, SPAN), BF16),
            vmem((2 * rows, width), F32),
            vmem((2 * rows, SPAN), F32),
            vmem((ntp, rows, width), BF16),
            vmem((rows, width), BF16),
            vmem((ntp, width, d), BF16),
            vmem((rows, d), F32),
            pltpu.SemaphoreType.REGULAR,
            dma((nsp + 1,)),
            dma((nsp + 1,)),
            dma((3 * chips,)),
            dma((ntp,)),
            dma((2 * ntp,)),
            dma((ntp,)),
            dma,
            dma,
            dma((nsp,)),
            dma,
            dma,
            dma,
            dma,
            dma,
        ],
        compiler_params=pltpu.CompilerParams(
            collective_id=0, has_side_effects=True, vmem_limit_bytes=40 * 1024 * 1024
        ),
    )(tokens, norm_gain.reshape(1, d), w_query, w_key, w_value, w_out, key_rate)


def solution(mesh):
    return jax.shard_map(
        on_device,
        mesh=mesh,
        in_specs=(
            P(("grp", "sp"), None),
            P(),
            P(None, "tp"),
            P(None, "tp"),
            P(None, "tp"),
            P("tp", None),
            P("tp", ("grp", "sp")),
        ),
        out_specs=P(("grp", "sp"), None),
        check_vma=False,
    )
```

time: 361 us -> 68.9 us (0.19)
  the two profiles are of different devices: /device:TPU:2016 before, /device:TPU:1896 now
where the time goes in v1:
time: 68.9 us; the launch traced here: 68.5 us
  Pallas kernels  61.2 us (89%)
  local copies, waits for them, and re-layouts  7.35 us (11%)
    pallas_call x1, Pallas kernels, on_device(): pl.pallas_call(functools.partial(layer, nsp, ntp, far), out_shape=jax.Sha...  61.2 us
    unnamed x15, local copies, waits for them, and re-layouts  7.35 us

profile of v1, /device:TPU:1896, one launch (start us, length us, event | category | flops | bytes accessed | tf_op | source)
XLA Modules:
  0.0 68.5 jit_solution(4694256581128493967)
XLA Ops:
  0.0 0.0 copy-start.6
  0.0 0.7 copy-done.6
  0.7 0.0 copy-start
  0.7 1.0 %copy-done = bf16[128,2048]{1,0:T(8,128)(2,1)S(1)} copy-done((bf16[128,2048]{1,0:T(8,128)(2,1)S(1)}, bf16[128,2048]{1,0:T(8,128)(2,1)}, u32[]{:S(2)}) %copy-start) | copy-done | bytes 524312
  1.7 0.0 copy-start.1
  1.7 1.0 %copy-done.1 = bf16[2048,128]{1,0:T(8,128)(2,1)S(1)} copy-done((bf16[2048,128]{1,0:T(8,128)(2,1)S(1)}, bf16[2048,128]{1,0:T(8,128)(2,1)}, u32[]{:S(2)}) %copy-start.1) | copy-done | bytes 524312
  2.7 0.0 copy-start.2
  2.7 1.0 %copy-done.2 = bf16[2048,128]{1,0:T(8,128)(2,1)S(1)} copy-done((bf16[2048,128]{1,0:T(8,128)(2,1)S(1)}, bf16[2048,128]{1,0:T(8,128)(2,1)}, u32[]{:S(2)}) %copy-start.2) | copy-done | bytes 524312
  3.8 0.0 copy-start.3
  3.8 1.0 %copy-done.3 = bf16[2048,128]{1,0:T(8,128)(2,1)S(1)} copy-done((bf16[2048,128]{1,0:T(8,128)(2,1)S(1)}, bf16[2048,128]{1,0:T(8,128)(2,1)}, u32[]{:S(2)}) %copy-start.3) | copy-done | bytes 524312
  4.8 0.0 copy-start.4
  4.8 1.0 %copy-done.4 = bf16[128,2048]{1,0:T(8,128)(2,1)S(1)} copy-done((bf16[128,2048]{1,0:T(8,128)(2,1)S(1)}, bf16[128,2048]{1,0:T(8,128)(2,1)}, u32[]{:S(2)}) %copy-start.4) | copy-done | bytes 524312
  5.9 0.0 copy-start.5
  5.9 0.7 %copy-done.5 = f32[2048]{0:T(1024)S(1)} copy-done((f32[2048]{0:T(1024)S(1)}, f32[2048]{0:T(1024)}, u32[]{:S(2)}) %copy-start.5) | copy-done | bytes 8216
  6.6 61.2 %shard_map.73 = bf16[128,2048]{1,0:T(8,128)(2,1)S(1)} custom-call(bf16[128,2048]{1,0:T(8,128)(2,1)S(1)} %copy-done, f32[1,2048]{1,0:T(1,128)S(1)} %bitcast.1, bf16[2048,128]{1,0:T(8,128)(2,1)S(1)} %copy-done.1, bf16[2048,128]{1,0:T(8,128)(2,1)S(1)} %copy-done.2, bf16[2048,128]{1,0:T(8,128)(2,1)S(1)} %copy-done.3, bf16[128,2048]{1,0:T(8,128)(2,1)S(1)} %copy-done.4, ...), custom_call_target="tpu_custom_call" | custom-call | tf_op jit(solution)/shard_map/pallas_call | solution.py:492
  67.7 0.8 %copy.9 = bf16[128,2048]{1,0:T(8,128)(2,1)} copy(bf16[128,2048]{1,0:T(8,128)(2,1)S(1)} %shard_map.73) | data formatting | bytes 1048576
Async XLA Ops:
  0.0 0.7 copy-start.6
  0.7 1.0 %copy-start = (bf16[128,2048]{1,0:T(8,128)(2,1)S(1)}, bf16[128,2048]{1,0:T(8,128)(2,1)}, u32[]{:S(2)}) copy-start(bf16[128,2048]{1,0:T(8,128)(2,1)} %tokens.1) | copy-start | bytes 1572868
  1.7 1.0 %copy-start.1 = (bf16[2048,128]{1,0:T(8,128)(2,1)S(1)}, bf16[2048,128]{1,0:T(8,128)(2,1)}, u32[]{:S(2)}) copy-start(bf16[2048,128]{1,0:T(8,128)(2,1)} %w_query.1) | copy-start | bytes 1572868
  2.7 1.0 %copy-start.2 = (bf16[2048,128]{1,0:T(8,128)(2,1)S(1)}, bf16[2048,128]{1,0:T(8,128)(2,1)}, u32[]{:S(2)}) copy-start(bf16[2048,128]{1,0:T(8,128)(2,1)} %w_key.1) | copy-start | bytes 1572868
  3.8 1.0 %copy-start.3 = (bf16[2048,128]{1,0:T(8,128)(2,1)S(1)}, bf16[2048,128]{1,0:T(8,128)(2,1)}, u32[]{:S(2)}) copy-start(bf16[2048,128]{1,0:T(8,128)(2,1)} %w_value.1) | copy-start | bytes 1572868
  4.8 1.0 %copy-start.4 = (bf16[128,2048]{1,0:T(8,128)(2,1)S(1)}, bf16[128,2048]{1,0:T(8,128)(2,1)}, u32[]{:S(2)}) copy-start(bf16[128,2048]{1,0:T(8,128)(2,1)} %w_out.1) | copy-start | bytes 1572868
  5.9 0.7 %copy-start.5 = (f32[2048]{0:T(1024)S(1)}, f32[2048]{0:T(1024)}, u32[]{:S(2)}) copy-start(f32[2048]{0:T(1024)} %param.8) | copy-start | bytes 24580

commit v2 on v1

v2 whole, which is shorter than its diff:
```python
import functools

import jax
import jax.numpy as jnp
from jax import lax
from jax.experimental import pallas as pl
from jax.experimental.pallas import tpu as pltpu
from jax.sharding import PartitionSpec as P

HD = 64
SPAN = 128
PAD = 16
VAL = SPAN + PAD
CHUNKS = ((0, VAL), (VAL, SPAN))

F32 = jnp.float32
BF16 = jnp.bfloat16
EPS = 1e-06
MESH = pl.DeviceIdType.MESH


def dot(a, b):
    return lax.dot_general(a, b, (((1,), (0,)), ((), ())), preferred_element_type=F32)


def dot_t(a, b):
    return lax.dot_general(a, b, (((1,), (1,)), ((), ())), preferred_element_type=F32)


def layer(
    nsp,
    ntp,
    far,
    tokens_hbm,
    gain,
    w_query_hbm,
    w_key_hbm,
    w_value_hbm,
    w_out_hbm,
    rate,
    out,
    tokens,
    w_query,
    w_key,
    w_value,
    w_out,
    kv,
    normed,
    other_tokens,
    queries,
    first_q,
    first_queries,
    far_sent,
    far_in,
    far_queries,
    far_back,
    far_got,
    tri,
    rate_now,
    late_rate,
    acc,
    past,
    other_acc,
    other_past,
    mixed,
    first_mixed,
    w_all,
    total,
    late_sem,
    load,
    kv_send,
    kv_recv,
    down_send,
    w_send,
    lent_send,
    w_recv,
    mx_send,
    first_send,
    mx_recv,
    tok_send,
    tok_recv,
    lr_send,
    lr_recv,
    h_send,
    h_recv,
    fq_send,
    fq_recv,
    fa_send,
    fa_recv,
    out_send,
    out_recv,
):
    z = lax.axis_index("sp")
    t = lax.axis_index("tp")
    chips = ntp // 2
    x, core = t // 2, lax.rem(t, 2)
    sibling = 2 * x + 1 - core
    reach = nsp - 1 - far
    lead = t == 0
    first = z == 0
    last = z == nsp - 1
    outset = jnp.logical_and(first, lead)
    deputy = jnp.logical_and(z == 1, lead)
    helper = jnp.logical_and(first, t == 1)
    host = jnp.logical_and(z >= 1, z <= reach)
    guest = z > far

    bar = pltpu.get_barrier_semaphore()

    def at(zz, tt):
        return {"sp": zz, "tp": tt}

    def greet(zz, tt):
        pl.semaphore_signal(bar, inc=1, device_id=at(zz, tt), device_id_type=MESH)

    def send(src, dst, ss, rs, zz, tt):
        return pltpu.make_async_remote_copy(
            src_ref=src, dst_ref=dst, send_sem=ss, recv_sem=rs, device_id=at(zz, tt), device_id_type=MESH
        )

    loads = [
        pltpu.make_async_copy(a, b, load.at[i])
        for i, (a, b) in enumerate(
            (
                (tokens_hbm, tokens),
                (w_key_hbm, w_key),
                (w_value_hbm, w_value),
                (w_query_hbm, w_query),
                (w_out_hbm, w_out),
            )
        )
    ]

    @pl.when(jnp.logical_not(outset))
    def _():
        for c in loads:
            c.start()

    @pl.when(jnp.logical_and(z >= 1, core == 1))
    def _():
        greet(z - 1, t)

    for p in range(ntp):

        @pl.when(jnp.logical_and(t != 0, t != p))
        def _():
            greet(z, p)

    @pl.when(host)
    def _():
        greet(z + far, t)

    @pl.when(jnp.logical_and(host, lead))
    def _():
        greet(0, 0)

    @pl.when(jnp.logical_and(first, t != 0))
    def _():
        greet(1, 0)

    @pl.when(deputy)
    def _():
        greet(0, 1)

    one = lambda flag: jnp.where(flag, 1, 0)
    expected = (
        one(jnp.logical_and(jnp.logical_not(last), core == 1))
        + jnp.where(lead, ntp - 1, ntp - 2)
        + one(guest)
        + one(outset) * reach
        + one(deputy) * (ntp - 1)
        + one(helper)
    )

    @pl.when(jnp.logical_not(outset))
    def _():
        row = lax.broadcasted_iota(jnp.int32, (2 * SPAN, 2 * SPAN), 0)
        col = lax.broadcasted_iota(jnp.int32, (2 * SPAN, 2 * SPAN), 1)
        later = jnp.logical_or(col >= SPAN, lax.rem(row, SPAN) >= col)
        tri[...] = jnp.where(later, 1.0, 0.0).astype(BF16)

    def split_heads(dst, q):
        lane = lax.broadcasted_iota(jnp.int32, (SPAN, 2 * HD), 1)
        qf = q.astype(F32)
        dst[:SPAN] = jnp.where(lane < HD, qf, 0.0).astype(BF16)
        dst[SPAN:] = jnp.where(lane >= HD, qf, 0.0).astype(BF16)

    def join_heads(a):
        lane = lax.broadcasted_iota(jnp.int32, (SPAN, 2 * HD), 1)
        return jnp.where(lane < HD, a[:SPAN], a[SPAN:])

    def project(src, slot, wait):
        wait(0)
        xs = src[...].astype(F32)
        scale = lax.rsqrt(jnp.mean(xs * xs, axis=-1, keepdims=True) + EPS)
        normed[...] = (xs * scale * gain[...]).astype(BF16)
        wait(1)
        kv[slot, core, pl.ds(0, SPAN)] = dot(normed[...], w_key[...]).astype(BF16)
        wait(2)
        kv[slot, core, pl.ds(VAL, SPAN)] = dot(normed[...], w_value[...]).astype(BF16)
        kv[slot, core, pl.ds(SPAN, PAD)] = jnp.concatenate(
            [rate[...].astype(F32), jnp.zeros((PAD - 2, SPAN), F32)], axis=0
        ).astype(BF16)
        wait(3)
        return dot(normed[...], w_query[...]).astype(BF16) * HD ** (-0.5)

    def attend(q_ref, slot, diagonal, acc=acc, past=past, part=core):
        s = dot_t(q_ref[...], kv[slot, part, pl.ds(0, SPAN)])
        s = jnp.concatenate([s[:SPAN] + rate_now[0:1], s[SPAN:] + rate_now[1:2]], axis=0)
        soft = jnp.maximum(s, 0.0) + jnp.log(1.0 + jnp.exp(-jnp.abs(s)))
        if diagonal:
            r = lax.rem(lax.broadcasted_iota(jnp.int32, (2 * SPAN, SPAN), 0), SPAN)
            c = lax.broadcasted_iota(jnp.int32, (2 * SPAN, SPAN), 1)
            seen = c < r
            soft = jnp.where(seen, soft, 0.0)
        high = soft.astype(BF16)
        low = (soft - high.astype(F32)).astype(BF16)
        sums = dot(jnp.concatenate([high, low], axis=1), tri[...])
        weight = jnp.exp(s - sums[:, :SPAN])
        if diagonal:
            weight = jnp.where(seen, weight, 0.0)
        got = dot(weight.astype(BF16), kv[slot, part, pl.ds(VAL, SPAN)])
        if diagonal:
            acc[...] = got
            past[...] = sums[:, SPAN:]
        else:
            acc[...] = acc[...] + jnp.exp(-past[...]) * got
            past[...] = past[...] + sums[:, SPAN:]

    def slab_rate(slot):
        rate_now[...] = kv[slot, core, pl.ds(SPAN, PAD)][:2].astype(F32)

    @pl.when(jnp.logical_not(outset))
    def _():
        q = project(tokens, 0, lambda i: loads[i].wait())
        far_sent[...] = q
        split_heads(queries, q)
        slab_rate(0)
        loads[4].wait()

    pl.semaphore_wait(bar, expected)

    late_rates = [send(rate, late_rate, lr_send.at[0], lr_recv, 0, 1)] + [
        send(rate, late_rate, lr_send.at[1], lr_recv, i, 0) for i in range(1, reach + 1)
    ]
    borrowed = send(tokens, other_tokens, tok_send, tok_recv, 1, 0)

    def w_copy(src, slot, sem, zz, tt):
        return send(src, w_all.at[slot], sem, w_recv.at[slot], zz, tt)

    def across(d):
        return 2 * lax.rem(x + d, chips) + core

    directs = [w_copy(w_out, t, w_send, z, across(d)) for d in range(1, chips)]
    to_sibling = w_copy(w_out, t, w_send, z, sibling)
    passed = [w_copy(w_all.at[across(d)], across(d), w_send, z, sibling) for d in range(1, chips)]
    lent = [w_copy(w_out, 0, lent_send, 0, p) for p in [1] + list(range(2, ntp, 2))]
    to_helper = w_copy(w_out, t, w_send, 0, 1)

    def up(k):
        return [
            send(kv.at[k, :, pl.ds(a, n)], kv.at[k + 1, :, pl.ds(a, n)], kv_send, kv_recv.at[k + 1, c], z + 1, t)
            for c, (a, n) in enumerate(CHUNKS)
        ]

    def down(k):
        return send(kv.at[k, 0], kv.at[k, 0], down_send, kv_recv.at[k, 0], z, sibling)

    def aside(k):
        return send(kv.at[k, 0], kv.at[k, 0], kv_send, kv_recv.at[k, 0], z, sibling)

    alone = send(kv.at[0, 1], kv.at[1, 1], kv_send, kv_recv.at[1, 1], 1, 1)
    back = [
        send(kv.at[1, 0], kv.at[1, 0], h_send.at[0], h_recv.at[0], 0, 1),
        send(first_q, first_q, h_send.at[1], h_recv.at[1], 0, 1),
    ]

    def mx_copy(p):
        return send(mixed.at[t], mixed.at[t], mx_send, mx_recv.at[t], z, p)

    def first_copy(p):
        return send(first_mixed, mixed.at[0], first_send, mx_recv.at[0], 0, p)

    ask = send(far_sent, far_in, fq_send, fq_recv, z - far, t)
    answer = send(far_back, far_got, fa_send, fa_recv, z + far, t)

    first_order = list(range(4, min(6, ntp))) + [p for p in range(2, ntp) if p not in (4, 5)]

    received = jnp.where(z <= reach, z, far)
    forwarded = jnp.where(last, 0, jnp.where(z + 1 <= reach, z + 1, far))

    @pl.when(outset)
    def _():
        for c in late_rates:
            c.start()

    @pl.when(helper)
    def _():
        borrowed.start()

    @pl.when(helper)
    def _():
        alone.start()

    @pl.when(jnp.logical_and(jnp.logical_and(core == 0, jnp.logical_not(outset)), forwarded > 0))
    def _():
        aside(0).start()

    @pl.when(guest)
    def _():
        ask.start()

    for p in range(1, ntp):

        @pl.when(jnp.logical_and(lead, z > 0) if p > 1 else lead)
        def _():
            pl.semaphore_signal(late_sem, inc=1, device_id=at(z, p), device_id_type=MESH)

    @pl.when(jnp.logical_not(outset))
    def _():
        for d in range(1, chips):

            @pl.when(across(d) != 0)
            def _():
                directs[d - 1].start()

        @pl.when(sibling != 0)
        def _():
            to_sibling.start()

    @pl.when(deputy)
    def _():
        for c in lent:
            c.start()

    @pl.when(jnp.logical_and(first, jnp.logical_and(core == 0, t != 0)))
    def _():
        to_helper.start()

    def to_lead():
        pl.semaphore_wait(late_sem, 1)
        for d in range(1, chips):

            @pl.when(across(d) == 0)
            def _():
                directs[d - 1].start()

        @pl.when(sibling == 0)
        def _():
            to_sibling.start()

    @pl.when(jnp.logical_and(z > 0, t != 0))
    def _():
        to_lead()

    @pl.when(jnp.logical_not(outset))
    def _():
        w_all[t] = w_out[...]

    @pl.when(deputy)
    def _():
        borrowed.wait_recv()
        q = project(other_tokens, 1, lambda i: None)
        first_q[...] = q
        aside(1).start()
        for c in back:
            c.start()

    @pl.when(jnp.logical_and(jnp.logical_and(core == 1, forwarded > 0), jnp.logical_not(helper)))
    def _():
        aside(0).wait_recv()
        for c in up(0):
            c.start()

    @pl.when(jnp.logical_not(outset))
    def _():
        attend(queries, 0, True)

    def absorb(k, carry):
        beside = jnp.logical_and(z == 1, t == 1)

        @pl.when(jnp.logical_and(core == 1, jnp.logical_not(beside)))
        def _():
            for c in range(len(CHUNKS)):
                up(k - 1)[c].wait_recv()

                @pl.when(k < forwarded)
                def _():
                    up(k)[c].start()

            down(k).start()

        @pl.when(beside)
        def _():
            alone.wait_recv()
            aside(1).wait_recv()

            @pl.when(k < forwarded)
            def _():
                for c in up(1):
                    c.start()

        @pl.when(jnp.logical_and(core == 0, jnp.logical_not(deputy)))
        def _():
            down(k).wait_recv()

        reaches_first = jnp.logical_and(lead, k == z)

        @pl.when(reaches_first)
        def _():
            late_rates[0].wait_recv()
            rate_now[...] = late_rate[...].astype(F32)

        @pl.when(jnp.logical_not(reaches_first))
        def _():
            slab_rate(k)

        @pl.when(k <= far)
        def _():
            attend(queries, k, False)

        return carry

    lax.fori_loop(1, received + 1, absorb, 0)

    @pl.when(host)
    def _():
        ask.wait_recv()
        split_heads(far_queries, far_in[...])
        other_acc[...] = jnp.zeros_like(other_acc)
        other_past[...] = jnp.zeros_like(other_past)

        def absorb_far(k, carry):
            reaches_first = jnp.logical_and(lead, k == z)

            @pl.when(reaches_first)
            def _():
                rate_now[...] = late_rate[...].astype(F32)

            @pl.when(jnp.logical_not(reaches_first))
            def _():
                slab_rate(k)

            attend(far_queries, k, False, other_acc, other_past)
            return carry

        lax.fori_loop(1, z + 1, absorb_far, 0)
        far_back[...] = join_heads(other_acc[...]).astype(BF16)
        answer.start()

    @pl.when(guest)
    def _():
        answer.wait_recv()
        acc[...] = acc[...] + jnp.exp(-past[...]) * jnp.concatenate([far_got[...].astype(F32)] * 2, axis=0)

    @pl.when(jnp.logical_not(outset))
    def _():
        mixed[t] = join_heads(acc[...]).astype(BF16)

    @pl.when(jnp.logical_not(outset))
    def _():
        for p in range(1, ntp):

            @pl.when(t != p)
            def _():
                mx_copy(p).start()

    @pl.when(jnp.logical_and(z > 0, t != 0))
    def _():
        mx_copy(0).start()

    for d in range(1, chips):

        @pl.when(jnp.logical_not(outset))
        def _():
            w_copy(w_out, across(d), w_send, z, t).wait_recv()

        @pl.when(jnp.logical_not(jnp.logical_and(first, x == 0)))
        def _():
            passed[d - 1].start()

    @pl.when(helper)
    def _():
        for c in back:
            c.wait_recv()
        split_heads(first_queries, first_q[...])
        late_rates[0].wait_recv()
        rate_now[...] = late_rate[...].astype(F32)
        attend(first_queries, 1, True, other_acc, other_past, 0)
        first_mixed[...] = join_heads(other_acc[...]).astype(BF16)
        for p in first_order:
            first_copy(p).start()
        mixed[0] = first_mixed[...]

    def wait_w(slot):
        w_copy(w_out, slot, w_send, z, t).wait_recv()

    def wait_mixed(slot):
        send(mixed.at[slot], mixed.at[slot], mx_send, mx_recv.at[slot], z, t).wait_recv()

    @pl.when(jnp.logical_not(outset))
    def _():
        for xx in list(range(1, chips)) + [0]:
            for slot in (2 * xx, 2 * xx + 1):
                pl.when(core != slot % 2)(functools.partial(wait_w, slot))
                pl.when(jnp.logical_and(t != slot, jnp.logical_not(helper)) if slot == 0 else t != slot)(
                    functools.partial(wait_mixed, slot)
                )
            pair = jnp.concatenate([mixed[2 * xx], mixed[2 * xx + 1]], axis=1)
            rows = jnp.concatenate([w_all[2 * xx], w_all[2 * xx + 1]], axis=0)
            part = dot(pair, rows)
            if xx == 1 or chips == 1:
                total[...] = part
            elif xx > 0:
                total[...] = total[...] + part
            if xx == 0:
                out[...] = (total[...] + part if chips > 1 else part).astype(BF16)

    handed = send(out, out, out_send, out_recv, z, sibling)

    @pl.when(helper)
    def _():
        pl.semaphore_wait(late_sem, 1)
        handed.start()
        handed.wait_send()

    @pl.when(outset)
    def _():
        handed.wait_recv()

    def left(ref, sem):
        send(ref, ref, sem, out_recv, z, sibling).wait_send()

    @pl.when(outset)
    def _():
        left(rate, lr_send.at[0])
        left(kv.at[0, 0, pl.ds(0, 2 * reach)], lr_send.at[1])

    @pl.when(helper)
    def _():
        borrowed.wait_send()
        alone.wait_send()
        if chips > 1:
            left(w_all.at[pl.ds(0, chips - 1)], w_send)
        if ntp > 2:
            left(mixed.at[pl.ds(0, ntp - 2)], first_send)

    carrier = jnp.logical_and(core == 1, jnp.logical_not(helper))
    for n in range(1, reach + 2):

        @pl.when(jnp.logical_and(carrier, forwarded == n))
        def _():
            left(kv.at[pl.ds(0, n)], kv_send)

        if n <= reach:

            @pl.when(jnp.logical_and(jnp.logical_and(core == 1, received == n), jnp.logical_not(jnp.logical_and(z == 1, t == 1))))
            def _():
                left(kv.at[pl.ds(0, n), 0], down_send)

    @pl.when(jnp.logical_and(jnp.logical_and(core == 0, jnp.logical_not(outset)), forwarded > 0))
    def _():
        pl.when(deputy)(lambda: left(kv.at[0], kv_send))
        pl.when(jnp.logical_not(deputy))(lambda: left(kv.at[0, 0], kv_send))

    @pl.when(jnp.logical_not(jnp.logical_and(first, x == 0)))
    def _():
        left(w_all.at[pl.ds(0, ntp - 1)], w_send)

    @pl.when(z > 0)
    def _():
        left(mixed.at[pl.ds(0, ntp - 1)], mx_send)

    if ntp > 2:

        @pl.when(jnp.logical_and(first, t != 0))
        def _():
            left(mixed.at[pl.ds(0, ntp - 2)], mx_send)

    @pl.when(deputy)
    def _():
        left(w_all.at[pl.ds(0, chips)], lent_send)
        for c in back:
            c.wait_send()

    @pl.when(guest)
    def _():
        ask.wait_send()

    @pl.when(host)
    def _():
        answer.wait_send()


def on_device(tokens, norm_gain, w_query, w_key, w_value, w_out, key_rate):
    nsp, ntp = lax.axis_size("sp"), lax.axis_size("tp")
    rows, d = tokens.shape
    width = w_query.shape[1]
    far = nsp // 2 - 1
    chips = ntp // 2
    dma = pltpu.SemaphoreType.DMA
    vmem = pltpu.VMEM
    return pl.pallas_call(
        functools.partial(layer, nsp, ntp, far),
        out_shape=jax.ShapeDtypeStruct((rows, d), BF16),
        in_specs=[pl.BlockSpec(memory_space=pltpu.VMEM if i in (1, 6) else pltpu.HBM) for i in range(7)],
        out_specs=pl.BlockSpec(memory_space=pltpu.VMEM),
        scratch_shapes=[
            vmem((rows, d), BF16),
            vmem((d, width), BF16),
            vmem((d, width), BF16),
            vmem((d, width), BF16),
            vmem((width, d), BF16),
            vmem((nsp - far + 1, 2, 2 * SPAN + PAD, width), BF16),
            vmem((rows, d), BF16),
            vmem((rows, d), BF16),
            vmem((2 * rows, width), BF16),
            vmem((rows, width), BF16),
            vmem((2 * rows, width), BF16),
            vmem((rows, width), BF16),
            vmem((rows, width), BF16),
            vmem((2 * rows, width), BF16),
            vmem((rows, width), BF16),
            vmem((rows, width), BF16),
            vmem((2 * SPAN, 2 * SPAN), BF16),
            vmem((2, SPAN), F32),
            vmem((2, SPAN), BF16),
            vmem((2 * rows, width), F32),
            vmem((2 * rows, SPAN), F32),
            vmem((2 * rows, width), F32),
            vmem((2 * rows, SPAN), F32),
            vmem((ntp, rows, width), BF16),
            vmem((rows, width), BF16),
            vmem((ntp, width, d), BF16),
            vmem((rows, d), F32),
            pltpu.SemaphoreType.REGULAR,
            dma((5,)),
            dma,
            dma((nsp - far + 1, len(CHUNKS))),
            dma,
            dma,
            dma,
            dma((ntp,)),
            dma,
            dma,
            dma((ntp,)),
            dma,
            dma,
            dma((2,)),
            dma,
            dma((2,)),
            dma((2,)),
            dma,
            dma,
            dma,
            dma,
            dma,
            dma,
        ],
        compiler_params=pltpu.CompilerParams(
            collective_id=0, has_side_effects=True, vmem_limit_bytes=60 * 1024 * 1024
        ),
    )(tokens, norm_gain.reshape(1, d), w_query, w_key, w_value, w_out, key_rate)


def solution(mesh):
    return jax.shard_map(
        on_device,
        mesh=mesh,
        in_specs=(
            P(("grp", "sp"), None),
            P(),
            P(None, "tp"),
            P(None, "tp"),
            P(None, "tp"),
            P("tp", None),
            P("tp", ("grp", "sp")),
        ),
        out_specs=P(("grp", "sp"), None),
        check_vma=False,
    )
```

time: 68.9 us -> 58.2 us (0.84)
  the two profiles are of different devices: /device:TPU:1896 before, /device:TPU:2016 now
where the time goes in v2:
time: 58.2 us; the launch traced here: 57.8 us
  Pallas kernels  55.9 us (96%)
  local copies, waits for them, and re-layouts  1.88 us (3%)
    pallas_call x1, Pallas kernels, on_device(): pl.pallas_call(functools.partial(layer, nsp, ntp, far), out_shape=jax.Sha...  55.9 us
    unnamed x1, local copies, waits for them, and re-layouts  1.88 us

profile of v2, /device:TPU:2016, one launch (start us, length us, event | category | flops | bytes accessed | tf_op | source)
XLA Modules:
  0.0 57.8 jit_solution(12072624411184430245)
XLA Ops:
  0.0 55.9 %shard_map.73 = bf16[128,2048]{1,0:T(8,128)(2,1)} custom-call(bf16[128,2048]{1,0:T(8,128)(2,1)} %tokens_hbm.1, f32[1,2048]{1,0:T(1,128)} %bitcast.1, bf16[2048,128]{1,0:T(8,128)(2,1)} %w_query_hbm.1, bf16[2048,128]{1,0:T(8,128)(2,1)} %w_key_hbm.1, bf16[2048,128]{1,0:T(8,128)(2,1)} %w_value_hbm.1, bf16[128,2048]{1,0:T(8,128)(2,1)} %w_out_hbm.1, ...), custom_call_target="tpu_custom_call" | custom-call | tf_op jit(solution)/shard_map/pallas_call | solution.py:603
  55.9 1.9 %copy.9 = bf16[128,2048]{1,0:T(8,128)(2,1)} copy(bf16[128,2048]{1,0:T(8,128)(2,1)} %shard_map.73) | data formatting | bytes 1048576

commit v3 on v2

--- a/solution.py
+++ b/solution.py
@@ -58,6 +58,7 @@
     tri,
     rate_now,
     late_rate,
+    late_span,
     acc,
     past,
     other_acc,
@@ -96,6 +97,7 @@
     x, core = t // 2, lax.rem(t, 2)
     sibling = 2 * x + 1 - core
     reach = nsp - 1 - far
+    most = max(far, reach)
     lead = t == 0
     first = z == 0
     last = z == nsp - 1
@@ -150,7 +152,7 @@
     def _():
         greet(z + far, t)
 
-    @pl.when(jnp.logical_and(host, lead))
+    @pl.when(jnp.logical_and(jnp.logical_and(z >= 1, z <= most), lead))
     def _():
         greet(0, 0)
 
@@ -167,7 +169,7 @@
         one(jnp.logical_and(jnp.logical_not(last), core == 1))
         + jnp.where(lead, ntp - 1, ntp - 2)
         + one(guest)
-        + one(outset) * reach
+        + one(outset) * most
         + one(deputy) * (ntp - 1)
         + one(helper)
     )
@@ -241,7 +243,7 @@
     pl.semaphore_wait(bar, expected)
 
     late_rates = [send(rate, late_rate, lr_send.at[0], lr_recv, 0, 1)] + [
-        send(rate, late_rate, lr_send.at[1], lr_recv, i, 0) for i in range(1, reach + 1)
+        send(rate, late_rate, lr_send.at[1], lr_recv, i, 0) for i in range(1, most + 1)
     ]
     borrowed = send(tokens, other_tokens, tok_send, tok_recv, 1, 0)
 
@@ -286,8 +288,11 @@
 
     first_order = list(range(4, min(6, ntp))) + [p for p in range(2, ntp) if p not in (4, 5)]
 
-    received = jnp.where(z <= reach, z, far)
-    forwarded = jnp.where(last, 0, jnp.where(z + 1 <= reach, z + 1, far))
+    def needed(zz):
+        return jnp.where(zz <= reach, zz, jnp.minimum(zz, far))
+
+    received = needed(z)
+    forwarded = jnp.where(last, 0, needed(z + 1))
 
     @pl.when(outset)
     def _():
@@ -423,6 +428,37 @@
 
     lax.fori_loop(1, received + 1, absorb, 0)
 
+    @pl.when(guest)
+    def _():
+        answer.wait_recv()
+        acc[...] = acc[...] + jnp.exp(-past[...]) * jnp.concatenate([far_got[...].astype(F32)] * 2, axis=0)
+
+    @pl.when(jnp.logical_not(outset))
+    def _():
+        mixed[t] = join_heads(acc[...]).astype(BF16)
+
+    @pl.when(jnp.logical_not(outset))
+    def _():
+        for p in range(1, ntp):
+
+            @pl.when(t != p)
+            def _():
+                mx_copy(p).start()
+
+    @pl.when(jnp.logical_and(z > 0, t != 0))
+    def _():
+        mx_copy(0).start()
+
+    for d in range(1, chips):
+
+        @pl.when(jnp.logical_not(outset))
+        def _():
+            w_copy(w_out, across(d), w_send, z, t).wait_recv()
+
+        @pl.when(jnp.logical_not(jnp.logical_and(first, x == 0)))
+        def _():
+            passed[d - 1].start()
+
     @pl.when(host)
     def _():
         ask.wait_recv()
@@ -448,36 +484,32 @@
         far_back[...] = join_heads(other_acc[...]).astype(BF16)
         answer.start()
 
-    @pl.when(guest)
-    def _():
-        answer.wait_recv()
-        acc[...] = acc[...] + jnp.exp(-past[...]) * jnp.concatenate([far_got[...].astype(F32)] * 2, axis=0)
-
-    @pl.when(jnp.logical_not(outset))
-    def _():
-        mixed[t] = join_heads(acc[...]).astype(BF16)
-
-    @pl.when(jnp.logical_not(outset))
-    def _():
-        for p in range(1, ntp):
-
-            @pl.when(t != p)
-            def _():
-                mx_copy(p).start()
-
-    @pl.when(jnp.logical_and(z > 0, t != 0))
-    def _():
-        mx_copy(0).start()
-
-    for d in range(1, chips):
-
-        @pl.when(jnp.logical_not(outset))
-        def _():
-            w_copy(w_out, across(d), w_send, z, t).wait_recv()
-
-        @pl.when(jnp.logical_not(jnp.logical_and(first, x == 0)))
-        def _():
-            passed[d - 1].start()
+    def wait_w(slot):
+        w_copy(w_out, slot, w_send, z, t).wait_recv()
+
+    def wait_mixed(slot):
+        send(mixed.at[slot], mixed.at[slot], mx_send, mx_recv.at[slot], z, t).wait_recv()
+
+    def project_out(xx):
+        for slot in (2 * xx, 2 * xx + 1):
+            pl.when(core != slot % 2)(functools.partial(wait_w, slot))
+            pl.when(jnp.logical_and(t != slot, jnp.logical_not(helper)) if slot == 0 else t != slot)(
+                functools.partial(wait_mixed, slot)
+            )
+        pair = jnp.concatenate([mixed[2 * xx], mixed[2 * xx + 1]], axis=1)
+        rows = jnp.concatenate([w_all[2 * xx], w_all[2 * xx + 1]], axis=0)
+        got = dot(pair, rows)
+        if xx == 1 and chips > 1:
+            total[...] = got
+        elif xx > 0:
+            total[...] = total[...] + got
+        else:
+            out[...] = (total[...] + got if chips > 1 else got).astype(BF16)
+
+    @pl.when(jnp.logical_not(outset))
+    def _():
+        for xx in range(1, chips):
+            project_out(xx)
 
     @pl.when(helper)
     def _():
@@ -492,29 +524,9 @@
             first_copy(p).start()
         mixed[0] = first_mixed[...]
 
-    def wait_w(slot):
-        w_copy(w_out, slot, w_send, z, t).wait_recv()
-
-    def wait_mixed(slot):
-        send(mixed.at[slot], mixed.at[slot], mx_send, mx_recv.at[slot], z, t).wait_recv()
-
-    @pl.when(jnp.logical_not(outset))
-    def _():
-        for xx in list(range(1, chips)) + [0]:
-            for slot in (2 * xx, 2 * xx + 1):
-                pl.when(core != slot % 2)(functools.partial(wait_w, slot))
-                pl.when(jnp.logical_and(t != slot, jnp.logical_not(helper)) if slot == 0 else t != slot)(
-                    functools.partial(wait_mixed, slot)
-                )
-            pair = jnp.concatenate([mixed[2 * xx], mixed[2 * xx + 1]], axis=1)
-            rows = jnp.concatenate([w_all[2 * xx], w_all[2 * xx + 1]], axis=0)
-            part = dot(pair, rows)
-            if xx == 1 or chips == 1:
-                total[...] = part
-            elif xx > 0:
-                total[...] = total[...] + part
-            if xx == 0:
-                out[...] = (total[...] + part if chips > 1 else part).astype(BF16)
+    @pl.when(jnp.logical_not(outset))
+    def _():
+        project_out(0)
 
     handed = send(out, out, out_send, out_recv, z, sibling)
 
@@ -534,7 +546,7 @@
     @pl.when(outset)
     def _():
         left(rate, lr_send.at[0])
-        left(kv.at[0, 0, pl.ds(0, 2 * reach)], lr_send.at[1])
+        left(late_span, lr_send.at[1])
 
     @pl.when(helper)
     def _():
@@ -546,17 +558,19 @@
             left(mixed.at[pl.ds(0, ntp - 2)], first_send)
 
     carrier = jnp.logical_and(core == 1, jnp.logical_not(helper))
-    for n in range(1, reach + 2):
+    for n in range(1, most + 1):
 
         @pl.when(jnp.logical_and(carrier, forwarded == n))
         def _():
             left(kv.at[pl.ds(0, n)], kv_send)
 
-        if n <= reach:
-
-            @pl.when(jnp.logical_and(jnp.logical_and(core == 1, received == n), jnp.logical_not(jnp.logical_and(z == 1, t == 1))))
-            def _():
-                left(kv.at[pl.ds(0, n), 0], down_send)
+        @pl.when(
+            jnp.logical_and(
+                jnp.logical_and(core == 1, received == n), jnp.logical_not(jnp.logical_and(z == 1, t == 1))
+            )
+        )
+        def _():
+            left(kv.at[pl.ds(0, n), 0], down_send)
 
     @pl.when(jnp.logical_and(jnp.logical_and(core == 0, jnp.logical_not(outset)), forwarded > 0))
     def _():
@@ -596,7 +610,8 @@
     nsp, ntp = lax.axis_size("sp"), lax.axis_size("tp")
     rows, d = tokens.shape
     width = w_query.shape[1]
-    far = nsp // 2 - 1
+    far = nsp // 2
+    most = max(far, nsp - 1 - far)
     chips = ntp // 2
     dma = pltpu.SemaphoreType.DMA
     vmem = pltpu.VMEM
@@ -611,7 +626,7 @@
             vmem((d, width), BF16),
             vmem((d, width), BF16),
             vmem((width, d), BF16),
-            vmem((nsp - far + 1, 2, 2 * SPAN + PAD, width), BF16),
+            vmem((most + 1, 2, 2 * SPAN + PAD, width), BF16),
             vmem((rows, d), BF16),
             vmem((rows, d), BF16),
             vmem((2 * rows, width), BF16),
@@ -625,6 +640,7 @@
             vmem((2 * SPAN, 2 * SPAN), BF16),
             vmem((2, SPAN), F32),
             vmem((2, SPAN), BF16),
+            vmem((most, 2, SPAN), BF16),
             vmem((2 * rows, width), F32),
             vmem((2 * rows, SPAN), F32),
             vmem((2 * rows, width), F32),
@@ -636,7 +652,7 @@
             pltpu.SemaphoreType.REGULAR,
             dma((5,)),
             dma,
-            dma((nsp - far + 1, len(CHUNKS))),
+            dma((most + 1, len(CHUNKS))),
             dma,
             dma,
             dma,

time: 58.2 us -> 52.5 us (0.902)
  the two profiles are of different devices: /device:TPU:2016 before, /device:TPU:168 now
where the time goes in v3:
time: 52.5 us; the launch traced here: 52.3 us
  Pallas kernels  50.4 us (96%)
  local copies, waits for them, and re-layouts  1.88 us (4%)
    pallas_call x1, Pallas kernels, on_device(): pl.pallas_call(functools.partial(layer, nsp, ntp, far), out_shape=jax.Sha...  50.4 us
    unnamed x1, local copies, waits for them, and re-layouts  1.88 us

profile of v3, /device:TPU:168, one launch (start us, length us, event | category | flops | bytes accessed | tf_op | source)
XLA Modules:
  0.0 52.3 jit_solution(8759890403396578549)
XLA Ops:
  0.0 50.4 %shard_map.73 = bf16[128,2048]{1,0:T(8,128)(2,1)} custom-call(bf16[128,2048]{1,0:T(8,128)(2,1)} %tokens_hbm.1, f32[1,2048]{1,0:T(1,128)} %bitcast.1, bf16[2048,128]{1,0:T(8,128)(2,1)} %w_query_hbm.1, bf16[2048,128]{1,0:T(8,128)(2,1)} %w_key_hbm.1, bf16[2048,128]{1,0:T(8,128)(2,1)} %w_value_hbm.1, bf16[128,2048]{1,0:T(8,128)(2,1)} %w_out_hbm.1, ...), custom_call_target="tpu_custom_call" | custom-call | tf_op jit(solution)/shard_map/pallas_call | solution.py:618
  50.4 1.9 %copy.9 = bf16[128,2048]{1,0:T(8,128)(2,1)} copy(bf16[128,2048]{1,0:T(8,128)(2,1)} %shard_map.73) | data formatting | bytes 1048576

commit v4 on v3

--- a/solution.py
+++ b/solution.py
@@ -174,6 +174,16 @@
         + one(helper)
     )
 
+    late_rates = [send(rate, late_rate, lr_send.at[0], lr_recv, 0, 1)] + [
+        send(rate, late_rate, lr_send.at[1], lr_recv, i, 0) for i in range(1, most + 1)
+    ]
+
+    @pl.when(outset)
+    def _():
+        pl.semaphore_wait(bar, expected)
+        for c in late_rates:
+            c.start()
+
     @pl.when(jnp.logical_not(outset))
     def _():
         row = lax.broadcasted_iota(jnp.int32, (2 * SPAN, 2 * SPAN), 0)
@@ -240,11 +250,10 @@
         slab_rate(0)
         loads[4].wait()
 
-    pl.semaphore_wait(bar, expected)
-
-    late_rates = [send(rate, late_rate, lr_send.at[0], lr_recv, 0, 1)] + [
-        send(rate, late_rate, lr_send.at[1], lr_recv, i, 0) for i in range(1, most + 1)
-    ]
+    @pl.when(jnp.logical_not(outset))
+    def _():
+        pl.semaphore_wait(bar, expected)
+
     borrowed = send(tokens, other_tokens, tok_send, tok_recv, 1, 0)
 
     def w_copy(src, slot, sem, zz, tt):
@@ -293,11 +302,6 @@
 
     received = needed(z)
     forwarded = jnp.where(last, 0, needed(z + 1))
-
-    @pl.when(outset)
-    def _():
-        for c in late_rates:
-            c.start()
 
     @pl.when(helper)
     def _():
@@ -370,119 +374,6 @@
         aside(1).start()
         for c in back:
             c.start()
-
-    @pl.when(jnp.logical_and(jnp.logical_and(core == 1, forwarded > 0), jnp.logical_not(helper)))
-    def _():
-        aside(0).wait_recv()
-        for c in up(0):
-            c.start()
-
-    @pl.when(jnp.logical_not(outset))
-    def _():
-        attend(queries, 0, True)
-
-    def absorb(k, carry):
-        beside = jnp.logical_and(z == 1, t == 1)
-
-        @pl.when(jnp.logical_and(core == 1, jnp.logical_not(beside)))
-        def _():
-            for c in range(len(CHUNKS)):
-                up(k - 1)[c].wait_recv()
-
-                @pl.when(k < forwarded)
-                def _():
-                    up(k)[c].start()
-
-            down(k).start()
-
-        @pl.when(beside)
-        def _():
-            alone.wait_recv()
-            aside(1).wait_recv()
-
-            @pl.when(k < forwarded)
-            def _():
-                for c in up(1):
-                    c.start()
-
-        @pl.when(jnp.logical_and(core == 0, jnp.logical_not(deputy)))
-        def _():
-            down(k).wait_recv()
-
-        reaches_first = jnp.logical_and(lead, k == z)
-
-        @pl.when(reaches_first)
-        def _():
-            late_rates[0].wait_recv()
-            rate_now[...] = late_rate[...].astype(F32)
-
-        @pl.when(jnp.logical_not(reaches_first))
-        def _():
-            slab_rate(k)
-
-        @pl.when(k <= far)
-        def _():
-            attend(queries, k, False)
-
-        return carry
-
-    lax.fori_loop(1, received + 1, absorb, 0)
-
-    @pl.when(guest)
-    def _():
-        answer.wait_recv()
-        acc[...] = acc[...] + jnp.exp(-past[...]) * jnp.concatenate([far_got[...].astype(F32)] * 2, axis=0)
-
-    @pl.when(jnp.logical_not(outset))
-    def _():
-        mixed[t] = join_heads(acc[...]).astype(BF16)
-
-    @pl.when(jnp.logical_not(outset))
-    def _():
-        for p in range(1, ntp):
-
-            @pl.when(t != p)
-            def _():
-                mx_copy(p).start()
-
-    @pl.when(jnp.logical_and(z > 0, t != 0))
-    def _():
-        mx_copy(0).start()
-
-    for d in range(1, chips):
-
-        @pl.when(jnp.logical_not(outset))
-        def _():
-            w_copy(w_out, across(d), w_send, z, t).wait_recv()
-
-        @pl.when(jnp.logical_not(jnp.logical_and(first, x == 0)))
-        def _():
-            passed[d - 1].start()
-
-    @pl.when(host)
-    def _():
-        ask.wait_recv()
-        split_heads(far_queries, far_in[...])
-        other_acc[...] = jnp.zeros_like(other_acc)
-        other_past[...] = jnp.zeros_like(other_past)
-
-        def absorb_far(k, carry):
-            reaches_first = jnp.logical_and(lead, k == z)
-
-            @pl.when(reaches_first)
-            def _():
-                rate_now[...] = late_rate[...].astype(F32)
-
-            @pl.when(jnp.logical_not(reaches_first))
-            def _():
-                slab_rate(k)
-
-            attend(far_queries, k, False, other_acc, other_past)
-            return carry
-
-        lax.fori_loop(1, z + 1, absorb_far, 0)
-        far_back[...] = join_heads(other_acc[...]).astype(BF16)
-        answer.start()
 
     def wait_w(slot):
         w_copy(w_out, slot, w_send, z, t).wait_recv()
@@ -506,10 +397,133 @@
         else:
             out[...] = (total[...] + got if chips > 1 else got).astype(BF16)
 
-    @pl.when(jnp.logical_not(outset))
+    def pass_on():
+        for d in range(1, chips):
+
+            @pl.when(jnp.logical_not(outset))
+            def _():
+                w_copy(w_out, across(d), w_send, z, t).wait_recv()
+
+            @pl.when(jnp.logical_not(jnp.logical_and(first, x == 0)))
+            def _():
+                passed[d - 1].start()
+
+    early = jnp.logical_and(lead, jnp.logical_and(z >= 1, z <= most))
+
+    @pl.when(jnp.logical_and(jnp.logical_and(core == 1, forwarded > 0), jnp.logical_not(helper)))
+    def _():
+        aside(0).wait_recv()
+        for c in up(0):
+            c.start()
+
+    @pl.when(jnp.logical_not(outset))
+    def _():
+        attend(queries, 0, True)
+
+    def absorb(k, carry):
+        beside = jnp.logical_and(z == 1, t == 1)
+
+        @pl.when(jnp.logical_and(core == 1, jnp.logical_not(beside)))
+        def _():
+            for c in range(len(CHUNKS)):
+                up(k - 1)[c].wait_recv()
+
+                @pl.when(k < forwarded)
+                def _():
+                    up(k)[c].start()
+
+            down(k).start()
+
+        @pl.when(beside)
+        def _():
+            alone.wait_recv()
+            aside(1).wait_recv()
+
+            @pl.when(k < forwarded)
+            def _():
+                for c in up(1):
+                    c.start()
+
+        @pl.when(jnp.logical_and(core == 0, jnp.logical_not(deputy)))
+        def _():
+            down(k).wait_recv()
+
+        reaches_first = jnp.logical_and(lead, k == z)
+
+        @pl.when(reaches_first)
+        def _():
+            pass_on()
+            for xx in range(1, chips):
+                project_out(xx)
+            late_rates[0].wait_recv()
+            rate_now[...] = late_rate[...].astype(F32)
+
+        @pl.when(jnp.logical_not(reaches_first))
+        def _():
+            slab_rate(k)
+
+        @pl.when(k <= far)
+        def _():
+            attend(queries, k, False)
+
+        return carry
+
+    lax.fori_loop(1, received + 1, absorb, 0)
+
+    @pl.when(guest)
+    def _():
+        answer.wait_recv()
+        acc[...] = acc[...] + jnp.exp(-past[...]) * jnp.concatenate([far_got[...].astype(F32)] * 2, axis=0)
+
+    @pl.when(jnp.logical_not(outset))
+    def _():
+        mixed[t] = join_heads(acc[...]).astype(BF16)
+
+    @pl.when(jnp.logical_not(outset))
+    def _():
+        for d in sorted(range(1, chips), key=lambda d: -min(d, chips - d)):
+            for c in range(2):
+                p = 2 * lax.rem(x + d, chips) + c
+
+                @pl.when(jnp.logical_or(z > 0, p != 0))
+                def _():
+                    mx_copy(p).start()
+
+        @pl.when(jnp.logical_not(helper))
+        def _():
+            mx_copy(sibling).start()
+
+    pl.when(jnp.logical_not(early))(pass_on)
+
+    @pl.when(jnp.logical_not(jnp.logical_or(outset, early)))
     def _():
         for xx in range(1, chips):
             project_out(xx)
+
+    @pl.when(host)
+    def _():
+        ask.wait_recv()
+        split_heads(far_queries, far_in[...])
+        other_acc[...] = jnp.zeros_like(other_acc)
+        other_past[...] = jnp.zeros_like(other_past)
+
+        def absorb_far(k, carry):
+            reaches_first = jnp.logical_and(lead, k == z)
+
+            @pl.when(reaches_first)
+            def _():
+                rate_now[...] = late_rate[...].astype(F32)
+
+            @pl.when(jnp.logical_not(reaches_first))
+            def _():
+                slab_rate(k)
+
+            attend(far_queries, k, False, other_acc, other_past)
+            return carry
+
+        lax.fori_loop(1, z + 1, absorb_far, 0)
+        far_back[...] = join_heads(other_acc[...]).astype(BF16)
+        answer.start()
 
     @pl.when(helper)
     def _():
@@ -674,7 +688,7 @@
             dma,
         ],
         compiler_params=pltpu.CompilerParams(
-            collective_id=0, has_side_effects=True, vmem_limit_bytes=60 * 1024 * 1024
+            collective_id=0, has_side_effects=True, vmem_limit_bytes=55_650_000
         ),
     )(tokens, norm_gain.reshape(1, d), w_query, w_key, w_value, w_out, key_rate)
 

time: 52.5 us -> 51.3 us (0.977)
  the two profiles are of different devices: /device:TPU:168 before, /device:TPU:160 now
where the time goes in v4:
time: 51.3 us; the launch traced here: 51.2 us
  Pallas kernels  49 us (96%)
  local copies, waits for them, and re-layouts  2.15 us (4%)
    pallas_call x1, Pallas kernels, on_device(): pl.pallas_call(functools.partial(layer, nsp, ntp, far), out_shape=jax.Sha...  49 us
    unnamed x5, local copies, waits for them, and re-layouts  2.15 us

profile of v4, /device:TPU:160, one launch (start us, length us, event | category | flops | bytes accessed | tf_op | source)
XLA Modules:
  0.0 51.2 jit_solution(12688596685142339339)
XLA Ops:
  0.0 0.0 copy-start.1
  0.0 0.7 %copy-done.1 = bf16[2,128]{1,0:T(2,128)(2,1)S(1)} copy-done((bf16[2,128]{1,0:T(2,128)(2,1)S(1)}, bf16[2,128]{1,0:T(2,128)(2,1)}, u32[]{:S(2)}) %copy-start.1) | copy-done | bytes 536
  0.7 0.0 copy-start
  0.7 0.7 %copy-done = f32[2048]{0:T(1024)S(1)} copy-done((f32[2048]{0:T(1024)S(1)}, f32[2048]{0:T(1024)}, u32[]{:S(2)}) %copy-start) | copy-done | bytes 8216
  1.4 49.0 %shard_map.73 = bf16[128,2048]{1,0:T(8,128)(2,1)S(1)} custom-call(bf16[128,2048]{1,0:T(8,128)(2,1)} %tokens_hbm.1, f32[1,2048]{1,0:T(1,128)S(1)} %bitcast.1, bf16[2048,128]{1,0:T(8,128)(2,1)} %w_query_hbm.1, bf16[2048,128]{1,0:T(8,128)(2,1)} %w_key_hbm.1, bf16[2048,128]{1,0:T(8,128)(2,1)} %w_value_hbm.1, bf16[128,2048]{1,0:T(8,128)(2,1)} %w_out_hbm.1, ...), custom_call_target="tpu_custom_call" | custom-call | tf_op jit(solution)/shard_map/pallas_call | solution.py:632
  50.4 0.8 %copy.9 = bf16[128,2048]{1,0:T(8,128)(2,1)} copy(bf16[128,2048]{1,0:T(8,128)(2,1)S(1)} %shard_map.73) | data formatting | bytes 1048576
Async XLA Ops:
  0.0 0.7 %copy-start.1 = (bf16[2,128]{1,0:T(2,128)(2,1)S(1)}, bf16[2,128]{1,0:T(2,128)(2,1)}, u32[]{:S(2)}) copy-start(bf16[2,128]{1,0:T(2,128)(2,1)} %rate.1) | copy-start | bytes 1540
  0.7 0.7 %copy-start = (f32[2048]{0:T(1024)S(1)}, f32[2048]{0:T(1024)}, u32[]{:S(2)}) copy-start(f32[2048]{0:T(1024)} %param.8) | copy-start | bytes 24580

commit v5 on v4

--- a/solution.py
+++ b/solution.py
@@ -11,11 +11,12 @@
 SPAN = 128
 PAD = 16
 VAL = SPAN + PAD
-CHUNKS = ((0, VAL), (VAL, SPAN))
+CHUNKS = ((0, 96), (96, 80), (176, 96))
 
 F32 = jnp.float32
 BF16 = jnp.bfloat16
 EPS = 1e-06
+SKIP = 3
 MESH = pl.DeviceIdType.MESH
 
 
@@ -31,6 +32,7 @@
     nsp,
     ntp,
     far,
+    alone_to,
     tokens_hbm,
     gain,
     w_query_hbm,
@@ -68,6 +70,7 @@
     w_all,
     total,
     late_sem,
+    ready_sem,
     load,
     kv_send,
     kv_recv,
@@ -82,6 +85,7 @@
     tok_recv,
     lr_send,
     lr_recv,
+    relay_send,
     h_send,
     h_recv,
     fq_send,
@@ -97,15 +101,16 @@
     x, core = t // 2, lax.rem(t, 2)
     sibling = 2 * x + 1 - core
     reach = nsp - 1 - far
-    most = max(far, reach)
+    most = max(alone_to, reach)
+    near = min(nsp // 4, most)
     lead = t == 0
     first = z == 0
     last = z == nsp - 1
     outset = jnp.logical_and(first, lead)
     deputy = jnp.logical_and(z == 1, lead)
     helper = jnp.logical_and(first, t == 1)
-    host = jnp.logical_and(z >= 1, z <= reach)
-    guest = z > far
+    host = jnp.logical_and(z > alone_to - far, z <= reach)
+    guest = z > alone_to
 
     bar = pltpu.get_barrier_semaphore()
 
@@ -125,9 +130,9 @@
         for i, (a, b) in enumerate(
             (
                 (tokens_hbm, tokens),
+                (w_query_hbm, w_query),
                 (w_key_hbm, w_key),
                 (w_value_hbm, w_value),
-                (w_query_hbm, w_query),
                 (w_out_hbm, w_out),
             )
         )
@@ -152,7 +157,7 @@
     def _():
         greet(z + far, t)
 
-    @pl.when(jnp.logical_and(jnp.logical_and(z >= 1, z <= most), lead))
+    @pl.when(jnp.logical_and(jnp.logical_and(z >= 1, z <= near), lead))
     def _():
         greet(0, 0)
 
@@ -169,13 +174,13 @@
         one(jnp.logical_and(jnp.logical_not(last), core == 1))
         + jnp.where(lead, ntp - 1, ntp - 2)
         + one(guest)
-        + one(outset) * most
+        + one(outset) * near
         + one(deputy) * (ntp - 1)
         + one(helper)
     )
 
     late_rates = [send(rate, late_rate, lr_send.at[0], lr_recv, 0, 1)] + [
-        send(rate, late_rate, lr_send.at[1], lr_recv, i, 0) for i in range(1, most + 1)
+        send(rate, late_rate, lr_send.at[1], lr_recv, i, 0) for i in range(1, near + 1)
     ]
 
     @pl.when(outset)
@@ -201,20 +206,22 @@
         lane = lax.broadcasted_iota(jnp.int32, (SPAN, 2 * HD), 1)
         return jnp.where(lane < HD, a[:SPAN], a[SPAN:])
 
-    def project(src, slot, wait):
+    def project_queries(src, wait):
         wait(0)
         xs = src[...].astype(F32)
         scale = lax.rsqrt(jnp.mean(xs * xs, axis=-1, keepdims=True) + EPS)
         normed[...] = (xs * scale * gain[...]).astype(BF16)
         wait(1)
+        return dot(normed[...], w_query[...]).astype(BF16) * HD ** (-0.5)
+
+    def project_slab(slot, wait):
+        wait(2)
         kv[slot, core, pl.ds(0, SPAN)] = dot(normed[...], w_key[...]).astype(BF16)
-        wait(2)
+        wait(3)
         kv[slot, core, pl.ds(VAL, SPAN)] = dot(normed[...], w_value[...]).astype(BF16)
         kv[slot, core, pl.ds(SPAN, PAD)] = jnp.concatenate(
             [rate[...].astype(F32), jnp.zeros((PAD - 2, SPAN), F32)], axis=0
         ).astype(BF16)
-        wait(3)
-        return dot(normed[...], w_query[...]).astype(BF16) * HD ** (-0.5)
 
     def attend(q_ref, slot, diagonal, acc=acc, past=past, part=core):
         s = dot_t(q_ref[...], kv[slot, part, pl.ds(0, SPAN)])
@@ -242,17 +249,23 @@
     def slab_rate(slot):
         rate_now[...] = kv[slot, core, pl.ds(SPAN, PAD)][:2].astype(F32)
 
-    @pl.when(jnp.logical_not(outset))
-    def _():
-        q = project(tokens, 0, lambda i: loads[i].wait())
+    ask = send(far_sent, far_in, fq_send, fq_recv, z - far, t)
+    answer = send(far_back, far_got, fa_send, fa_recv, z + far, t)
+
+    @pl.when(jnp.logical_not(outset))
+    def _():
+        q = project_queries(tokens, lambda i: loads[i].wait())
         far_sent[...] = q
         split_heads(queries, q)
+        pl.semaphore_wait(bar, expected)
+
+        @pl.when(guest)
+        def _():
+            ask.start()
+
+        project_slab(0, lambda i: loads[i].wait())
         slab_rate(0)
         loads[4].wait()
-
-    @pl.when(jnp.logical_not(outset))
-    def _():
-        pl.semaphore_wait(bar, expected)
 
     borrowed = send(tokens, other_tokens, tok_send, tok_recv, 1, 0)
 
@@ -292,13 +305,10 @@
     def first_copy(p):
         return send(first_mixed, mixed.at[0], first_send, mx_recv.at[0], 0, p)
 
-    ask = send(far_sent, far_in, fq_send, fq_recv, z - far, t)
-    answer = send(far_back, far_got, fa_send, fa_recv, z + far, t)
-
     first_order = list(range(4, min(6, ntp))) + [p for p in range(2, ntp) if p not in (4, 5)]
 
     def needed(zz):
-        return jnp.where(zz <= reach, zz, jnp.minimum(zz, far))
+        return jnp.where(zz <= most, zz, far)
 
     received = needed(z)
     forwarded = jnp.where(last, 0, needed(z + 1))
@@ -314,10 +324,6 @@
     @pl.when(jnp.logical_and(jnp.logical_and(core == 0, jnp.logical_not(outset)), forwarded > 0))
     def _():
         aside(0).start()
-
-    @pl.when(guest)
-    def _():
-        ask.start()
 
     for p in range(1, ntp):
 
@@ -369,8 +375,8 @@
     @pl.when(deputy)
     def _():
         borrowed.wait_recv()
-        q = project(other_tokens, 1, lambda i: None)
-        first_q[...] = q
+        first_q[...] = project_queries(other_tokens, lambda i: None)
+        project_slab(1, lambda i: None)
         aside(1).start()
         for c in back:
             c.start()
@@ -408,7 +414,14 @@
             def _():
                 passed[d - 1].start()
 
-    early = jnp.logical_and(lead, jnp.logical_and(z >= 1, z <= most))
+    early = jnp.logical_and(lead, jnp.logical_and(z >= 1, z <= reach // 2))
+
+    relays = jnp.logical_and(lead, jnp.logical_and(z >= 1, z <= most - near))
+    relayed = send(late_rate, late_rate, relay_send, lr_recv, z + near, 0)
+
+    def relay():
+        pl.semaphore_wait(ready_sem, 1)
+        relayed.start()
 
     @pl.when(jnp.logical_and(jnp.logical_and(core == 1, forwarded > 0), jnp.logical_not(helper)))
     def _():
@@ -448,21 +461,29 @@
         def _():
             down(k).wait_recv()
 
+            @pl.when(jnp.logical_and(jnp.logical_and(lead, k == near), jnp.logical_and(z > near, z <= most)))
+            def _():
+                pl.semaphore_signal(ready_sem, inc=1, device_id=at(z - near, 0), device_id_type=MESH)
+
         reaches_first = jnp.logical_and(lead, k == z)
 
         @pl.when(reaches_first)
         def _():
-            pass_on()
-            for xx in range(1, chips):
-                project_out(xx)
+            @pl.when(early)
+            def _():
+                pass_on()
+                for xx in range(1, chips):
+                    project_out(xx)
+
             late_rates[0].wait_recv()
+            pl.when(jnp.logical_and(relays, z < near // 2))(relay)
             rate_now[...] = late_rate[...].astype(F32)
 
         @pl.when(jnp.logical_not(reaches_first))
         def _():
             slab_rate(k)
 
-        @pl.when(k <= far)
+        @pl.when(jnp.logical_or(k <= far, z <= alone_to))
         def _():
             attend(queries, k, False)
 
@@ -495,13 +516,7 @@
 
     pl.when(jnp.logical_not(early))(pass_on)
 
-    @pl.when(jnp.logical_not(jnp.logical_or(outset, early)))
-    def _():
-        for xx in range(1, chips):
-            project_out(xx)
-
-    @pl.when(host)
-    def _():
+    def serve():
         ask.wait_recv()
         split_heads(far_queries, far_in[...])
         other_acc[...] = jnp.zeros_like(other_acc)
@@ -524,6 +539,17 @@
         lax.fori_loop(1, z + 1, absorb_far, 0)
         far_back[...] = join_heads(other_acc[...]).astype(BF16)
         answer.start()
+
+    soon = z > reach // 2
+    pl.when(jnp.logical_and(host, soon))(serve)
+    pl.when(jnp.logical_and(relays, z >= near // 2))(relay)
+
+    @pl.when(jnp.logical_not(jnp.logical_or(outset, early)))
+    def _():
+        for xx in range(1, chips):
+            project_out(xx)
+
+    pl.when(jnp.logical_and(host, jnp.logical_not(soon)))(serve)
 
     @pl.when(helper)
     def _():
@@ -611,6 +637,10 @@
         for c in back:
             c.wait_send()
 
+    @pl.when(relays)
+    def _():
+        relayed.wait_send()
+
     @pl.when(guest)
     def _():
         ask.wait_send()
@@ -625,12 +655,13 @@
     rows, d = tokens.shape
     width = w_query.shape[1]
     far = nsp // 2
-    most = max(far, nsp - 1 - far)
+    alone_to = min(far + SKIP, nsp - 1)
+    most = max(alone_to, nsp - 1 - far)
     chips = ntp // 2
     dma = pltpu.SemaphoreType.DMA
     vmem = pltpu.VMEM
     return pl.pallas_call(
-        functools.partial(layer, nsp, ntp, far),
+        functools.partial(layer, nsp, ntp, far, alone_to),
         out_shape=jax.ShapeDtypeStruct((rows, d), BF16),
         in_specs=[pl.BlockSpec(memory_space=pltpu.VMEM if i in (1, 6) else pltpu.HBM) for i in range(7)],
         out_specs=pl.BlockSpec(memory_space=pltpu.VMEM),
@@ -654,7 +685,7 @@
             vmem((2 * SPAN, 2 * SPAN), BF16),
             vmem((2, SPAN), F32),
             vmem((2, SPAN), BF16),
-            vmem((most, 2, SPAN), BF16),
+            vmem((min(nsp // 4, most), 2, SPAN), BF16),
             vmem((2 * rows, width), F32),
             vmem((2 * rows, SPAN), F32),
             vmem((2 * rows, width), F32),
@@ -664,6 +695,7 @@
             vmem((ntp, width, d), BF16),
             vmem((rows, d), F32),
             pltpu.SemaphoreType.REGULAR,
+            pltpu.SemaphoreType.REGULAR,
             dma((5,)),
             dma,
             dma((most + 1, len(CHUNKS))),
@@ -677,6 +709,7 @@
             dma,
             dma,
             dma((2,)),
+            dma,
             dma,
             dma((2,)),
             dma((2,)),

time: 51.3 us -> 50.2 us (0.979)
  the two profiles are of different devices: /device:TPU:160 before, /device:TPU:1249 now
where the time goes in v5:
time: 50.2 us; the launch traced here: 50 us
  Pallas kernels  47.8 us (95%)
  local copies, waits for them, and re-layouts  2.15 us (4%)
    pallas_call x1, Pallas kernels, on_device(): pl.pallas_call(functools.partial(layer, nsp, ntp, far, alone_to), out_sha...  47.8 us
    unnamed x5, local copies, waits for them, and re-layouts  2.15 us

profile of v5, /device:TPU:1249, one launch (start us, length us, event | category | flops | bytes accessed | tf_op | source)
XLA Modules:
  0.0 50.0 jit_solution(5307098886552154034)
XLA Ops:
  0.0 0.0 copy-start.1
  0.0 0.7 %copy-done.1 = bf16[2,128]{1,0:T(2,128)(2,1)S(1)} copy-done((bf16[2,128]{1,0:T(2,128)(2,1)S(1)}, bf16[2,128]{1,0:T(2,128)(2,1)}, u32[]{:S(2)}) %copy-start.1) | copy-done | bytes 536
  0.7 0.0 copy-start
  0.7 0.7 %copy-done = f32[2048]{0:T(1024)S(1)} copy-done((f32[2048]{0:T(1024)S(1)}, f32[2048]{0:T(1024)}, u32[]{:S(2)}) %copy-start) | copy-done | bytes 8216
  1.4 47.8 %shard_map.73 = bf16[128,2048]{1,0:T(8,128)(2,1)S(1)} custom-call(bf16[128,2048]{1,0:T(8,128)(2,1)} %tokens_hbm.1, f32[1,2048]{1,0:T(1,128)S(1)} %bitcast.1, bf16[2048,128]{1,0:T(8,128)(2,1)} %w_query_hbm.1, bf16[2048,128]{1,0:T(8,128)(2,1)} %w_key_hbm.1, bf16[2048,128]{1,0:T(8,128)(2,1)} %w_value_hbm.1, bf16[128,2048]{1,0:T(8,128)(2,1)} %w_out_hbm.1, ...), custom_call_target="tpu_custom_call" | custom-call | tf_op jit(solution)/shard_map/pallas_call | solution.py:663
  49.2 0.8 %copy.9 = bf16[128,2048]{1,0:T(8,128)(2,1)} copy(bf16[128,2048]{1,0:T(8,128)(2,1)S(1)} %shard_map.73) | data formatting | bytes 1048576
Async XLA Ops:
  0.0 0.7 %copy-start.1 = (bf16[2,128]{1,0:T(2,128)(2,1)S(1)}, bf16[2,128]{1,0:T(2,128)(2,1)}, u32[]{:S(2)}) copy-start(bf16[2,128]{1,0:T(2,128)(2,1)} %rate.1) | copy-start | bytes 1540
  0.7 0.7 %copy-start = (f32[2048]{0:T(1024)S(1)}, f32[2048]{0:T(1024)}, u32[]{:S(2)}) copy-start(f32[2048]{0:T(1024)} %param.8) | copy-start | bytes 24580

commit v6 on v5

--- a/solution.py
+++ b/solution.py
@@ -257,13 +257,18 @@
         q = project_queries(tokens, lambda i: loads[i].wait())
         far_sent[...] = q
         split_heads(queries, q)
+
+        @pl.when(jnp.logical_not(guest))
+        def _():
+            project_slab(0, lambda i: loads[i].wait())
+
         pl.semaphore_wait(bar, expected)
 
         @pl.when(guest)
         def _():
             ask.start()
-
-        project_slab(0, lambda i: loads[i].wait())
+            project_slab(0, lambda i: loads[i].wait())
+
         slab_rate(0)
         loads[4].wait()
 

time: 50.2 us -> 49.4 us (0.984)
  the two profiles are of different devices: /device:TPU:1249 before, /device:TPU:1257 now
where the time goes in v6:
time: 49.4 us; the launch traced here: 49.2 us
  Pallas kernels  47.1 us (95%)
  local copies, waits for them, and re-layouts  2.15 us (4%)
    pallas_call x1, Pallas kernels, on_device(): pl.pallas_call(functools.partial(layer, nsp, ntp, far, alone_to), out_sha...  47.1 us
    unnamed x5, local copies, waits for them, and re-layouts  2.15 us

profile of v6, /device:TPU:1257, one launch (start us, length us, event | category | flops | bytes accessed | tf_op | source)
XLA Modules:
  0.0 49.2 jit_solution(11310104039013819604)
XLA Ops:
  0.0 0.0 copy-start.1
  0.0 0.7 %copy-done.1 = bf16[2,128]{1,0:T(2,128)(2,1)S(1)} copy-done((bf16[2,128]{1,0:T(2,128)(2,1)S(1)}, bf16[2,128]{1,0:T(2,128)(2,1)}, u32[]{:S(2)}) %copy-start.1) | copy-done | bytes 536
  0.7 0.0 copy-start
  0.7 0.7 %copy-done = f32[2048]{0:T(1024)S(1)} copy-done((f32[2048]{0:T(1024)S(1)}, f32[2048]{0:T(1024)}, u32[]{:S(2)}) %copy-start) | copy-done | bytes 8216
  1.4 47.1 %shard_map.73 = bf16[128,2048]{1,0:T(8,128)(2,1)S(1)} custom-call(bf16[128,2048]{1,0:T(8,128)(2,1)} %tokens_hbm.1, f32[1,2048]{1,0:T(1,128)S(1)} %bitcast.1, bf16[2048,128]{1,0:T(8,128)(2,1)} %w_query_hbm.1, bf16[2048,128]{1,0:T(8,128)(2,1)} %w_key_hbm.1, bf16[2048,128]{1,0:T(8,128)(2,1)} %w_value_hbm.1, bf16[128,2048]{1,0:T(8,128)(2,1)} %w_out_hbm.1, ...), custom_call_target="tpu_custom_call" | custom-call | tf_op jit(solution)/shard_map/pallas_call | solution.py:668
  48.4 0.8 %copy.9 = bf16[128,2048]{1,0:T(8,128)(2,1)} copy(bf16[128,2048]{1,0:T(8,128)(2,1)S(1)} %shard_map.73) | data formatting | bytes 1048576
Async XLA Ops:
  0.0 0.7 %copy-start.1 = (bf16[2,128]{1,0:T(2,128)(2,1)S(1)}, bf16[2,128]{1,0:T(2,128)(2,1)}, u32[]{:S(2)}) copy-start(bf16[2,128]{1,0:T(2,128)(2,1)} %rate.1) | copy-start | bytes 1540
  0.7 0.7 %copy-start = (f32[2048]{0:T(1024)S(1)}, f32[2048]{0:T(1024)}, u32[]{:S(2)}) copy-start(f32[2048]{0:T(1024)} %param.8) | copy-start | bytes 24580

commit v7 on v6

--- a/solution.py
+++ b/solution.py
@@ -9,9 +9,9 @@
 
 HD = 64
 SPAN = 128
-PAD = 16
-VAL = SPAN + PAD
-CHUNKS = ((0, 96), (96, 80), (176, 96))
+PAD = 8
+VAL = SPAN
+CHUNKS = ((0, 96), (96, 80), (176, 88))
 
 F32 = jnp.float32
 BF16 = jnp.bfloat16
@@ -219,7 +219,7 @@
         kv[slot, core, pl.ds(0, SPAN)] = dot(normed[...], w_key[...]).astype(BF16)
         wait(3)
         kv[slot, core, pl.ds(VAL, SPAN)] = dot(normed[...], w_value[...]).astype(BF16)
-        kv[slot, core, pl.ds(SPAN, PAD)] = jnp.concatenate(
+        kv[slot, core, pl.ds(2 * SPAN, PAD)] = jnp.concatenate(
             [rate[...].astype(F32), jnp.zeros((PAD - 2, SPAN), F32)], axis=0
         ).astype(BF16)
 
@@ -247,7 +247,7 @@
             past[...] = past[...] + sums[:, SPAN:]
 
     def slab_rate(slot):
-        rate_now[...] = kv[slot, core, pl.ds(SPAN, PAD)][:2].astype(F32)
+        rate_now[...] = kv[slot, core, pl.ds(2 * SPAN, PAD)][:2].astype(F32)
 
     ask = send(far_sent, far_in, fq_send, fq_recv, z - far, t)
     answer = send(far_back, far_got, fa_send, fa_recv, z + far, t)

time: 49.4 us -> 49.1 us (level)
  the two profiles are of different devices: /device:TPU:1257 before, /device:TPU:99 now
where the time goes in v7:
time: 49.1 us; the launch traced here: 48.9 us
  Pallas kernels  46.8 us (95%)
  local copies, waits for them, and re-layouts  2.15 us (4%)
    pallas_call x1, Pallas kernels, on_device(): pl.pallas_call(functools.partial(layer, nsp, ntp, far, alone_to), out_sha...  46.8 us
    unnamed x5, local copies, waits for them, and re-layouts  2.15 us

profile of v7, /device:TPU:99, one launch (start us, length us, event | category | flops | bytes accessed | tf_op | source)
XLA Modules:
  0.0 48.9 jit_solution(16064383540938909249)
XLA Ops:
  0.0 0.0 copy-start.1
  0.0 0.7 %copy-done.1 = bf16[2,128]{1,0:T(2,128)(2,1)S(1)} copy-done((bf16[2,128]{1,0:T(2,128)(2,1)S(1)}, bf16[2,128]{1,0:T(2,128)(2,1)}, u32[]{:S(2)}) %copy-start.1) | copy-done | bytes 536
  0.7 0.0 copy-start
  0.7 0.7 %copy-done = f32[2048]{0:T(1024)S(1)} copy-done((f32[2048]{0:T(1024)S(1)}, f32[2048]{0:T(1024)}, u32[]{:S(2)}) %copy-start) | copy-done | bytes 8216
  1.4 46.8 %shard_map.73 = bf16[128,2048]{1,0:T(8,128)(2,1)S(1)} custom-call(bf16[128,2048]{1,0:T(8,128)(2,1)} %tokens_hbm.1, f32[1,2048]{1,0:T(1,128)S(1)} %bitcast.1, bf16[2048,128]{1,0:T(8,128)(2,1)} %w_query_hbm.1, bf16[2048,128]{1,0:T(8,128)(2,1)} %w_key_hbm.1, bf16[2048,128]{1,0:T(8,128)(2,1)} %w_value_hbm.1, bf16[128,2048]{1,0:T(8,128)(2,1)} %w_out_hbm.1, ...), custom_call_target="tpu_custom_call" | custom-call | tf_op jit(solution)/shard_map/pallas_call | solution.py:668
  48.1 0.8 %copy.9 = bf16[128,2048]{1,0:T(8,128)(2,1)} copy(bf16[128,2048]{1,0:T(8,128)(2,1)S(1)} %shard_map.73) | data formatting | bytes 1048576
Async XLA Ops:
  0.0 0.7 %copy-start.1 = (bf16[2,128]{1,0:T(2,128)(2,1)S(1)}, bf16[2,128]{1,0:T(2,128)(2,1)}, u32[]{:S(2)}) copy-start(bf16[2,128]{1,0:T(2,128)(2,1)} %rate.1) | copy-start | bytes 1540
  0.7 0.7 %copy-start = (f32[2048]{0:T(1024)S(1)}, f32[2048]{0:T(1024)}, u32[]{:S(2)}) copy-start(f32[2048]{0:T(1024)} %param.8) | copy-start | bytes 24580
